TPU v7x, 32 devices: a whole 2x2x4 slice. The times are simulated.
32 devices in a mesh: grp: 2 (over y), sp: 4 (over z), tp: 4 (over x, core).
Axes of the slice: x: 2, y: 2, z: 4, core: 2. Of those that a mesh axis runs over, the one named last changes fastest.
Arguments:
- tokens_in: bfloat16 [2048, 2048], P(('grp', 'sp')), parts along dimension 0, may hold values from -6 to 6
- input_gain: float32 [2048], replicated, may hold values from 0.1 to 1.9
- w_query: bfloat16 [2048, 1024], P('sp', 'tp'), may hold values from -0.125 to 0.125
- w_key: bfloat16 [2048, 1024], P('sp', 'tp'), may hold values from -1 to 1
- w_value: bfloat16 [2048, 1024], P('sp', 'tp'), may hold values from -0.125 to 0.125
- w_gates: bfloat16 [2048, 32], P('sp', 'tp'), may hold values from -3 to 3
- w_glu_value: bfloat16 [2048, 1024], P('sp', 'tp'), may hold values from -0.125 to 0.125
- sigmoid_opener_matrix: bfloat16 [2048, 1024], P('sp', 'tp'), may hold values from -0.125 to 0.125
- log_decay: float32 [2048, 16], P(('grp', 'sp'), 'tp'), parts along dimension 0, may hold values from -1 to 0
- head_gain: float32 [128], replicated, may hold values from 0.1 to 1.9
- conv_kernel: float32 [31, 1024], P(None, 'tp'), may hold values from -12 to 12
- norm_gain: float32 [1024], P('tp'), may hold values from 0.1 to 1.9
- norm_shift: float32 [1024], P('tp'), may hold values from -3 to 3
- out_delta: bfloat16 [2048, 1024], P(None, 'tp'), may hold values from -0.125 to 0.125
- out_conv: bfloat16 [2048, 1024], P(None, 'tp'), may hold values from -0.125 to 0.125
Outputs:
- mixed: bfloat16 [2048, 2048], P(('grp', 'sp'), 'tp'), parts along dimension 0
There are 2 independent parts, one for each index of `grp`. A program takes and returns all parts, laid end to end along the dimension named above; an argument that names none is the same for every part. Nothing has to cross between parts.
All inputs are finite; a program needn't handle non-finite values.
Results may differ from a plain program's by a relative error of at most 0.015.
Values may be sent and summed in bfloat16 or wider, within the bound.
A program may use at most 64 MiB of HBM per device.

v0:
```python
import functools

import jax
import jax.numpy as jnp
from jax import lax
from jax.experimental import pallas as pl
from jax.experimental.pallas import tpu as pltpu
from jax.sharding import PartitionSpec as P

EPSILON = 1e-06
BETA_SHIFT = 6.0
HALO = 16
MESH = pl.DeviceIdType.MESH
F32 = jnp.float32
BF16 = jnp.bfloat16
NT = (((1,), (1,)), ((), ()))
TN = (((0,), (0,)), ((), ()))
NN = (((1,), (0,)), ((), ()))
KEY, GATE, VALUE, QUERY, GLU, OPEN = range(6)


def bdot(left, right, dims=NN):
    return lax.dot_general(
        left.astype(BF16), right.astype(BF16), dims, preferred_element_type=F32
    )


def each(count, action):
    if count <= 8:
        for step in range(count):
            action(step)
    else:
        def body(step, carry):
            action(step)
            return carry

        lax.fori_loop(0, count, body, 0)


def kernel(cfg, tok_h, gain, wk_h, wg_h, wv_h, wq_h, wa_h, wb_h, ld, ldt, hgain, ck, ng, ns, od_h, oc_h,
           out,
           tok, normed, wk, wg, wv, wq, wa, wb, od, oc,
           keys, vals, betas, cums, xinv, gaps, rhs, local_out, reads, maps, ends,
           chain_in, chain_out, glu, halo, pad, conv, stat_out, stat_in, conv_acc, part_out, part_in, pair_out, pair_in,
           local_sem, z_send, z_recv, y_send, y_recv, chain_send, chain_recv,
           halo_send, halo_recv, stat_send, stat_recv, part_send, part_recv, pair_send, pair_recv):
    n_grp, n_sp, n_tp, conv_total = cfg
    grp, sp, tp = lax.axis_index("grp"), lax.axis_index("sp"), lax.axis_index("tp")
    length, width = tok.shape
    rows = wk_h.shape[0]
    channels = wa.shape[1]
    head_width = hgain.shape[1]
    heads = wk.shape[1] // head_width
    share = (rows // 2) // 16 * 16 if n_grp == 2 else 0
    pulled = rows - share

    sources = (wk_h, wg_h, wv_h, wq_h, wa_h, wb_h)
    targets = (wk, wg, wv, wq, wa, wb)

    def block_of(w, index, start, count):
        if w == GATE:
            return targets[w].at[index]
        return targets[w].at[pl.ds(pl.multiple_of(index * rows + start, 16), count)]

    load_tok = pltpu.make_async_copy(tok_h, tok, local_sem.at[0])
    load_tok.start()
    own = [
        pltpu.make_async_copy(sources[w], block_of(w, sp, 0, rows), local_sem.at[1 + w])
        for w in range(6)
    ]
    for copy in own:
        copy.start()
    load_od = pltpu.make_async_copy(od_h, od, local_sem.at[7])
    load_oc = pltpu.make_async_copy(oc_h, oc, local_sem.at[8])

    barrier = pltpu.get_barrier_semaphore()

    def greet(axis, me, count):
        def one(step):
            pl.semaphore_signal(
                barrier, inc=1, device_id={axis: lax.rem(me + step + 1, count)}, device_id_type=MESH
            )

        each(count - 1, one)

    greet("sp", sp, n_sp)
    greet("tp", tp, n_tp)
    greet("grp", grp, n_grp)
    pl.semaphore_wait(barrier, n_sp + n_tp + n_grp - 3)

    def origin(side, d):
        return sp - d if side == 0 else sp + d

    def arrives(side, d):
        return sp - d >= 0 if side == 0 else sp + d < n_sp

    def leaves(side, d):
        if side == 0:
            return (sp - (d - 1) >= 0) & (sp < n_sp - 1)
        return (sp + (d - 1) < n_sp) & (sp > 0)

    def part_of(w, index, side_of):
        if w == GATE:
            return block_of(w, index, 0, 0)
        if not share:
            return block_of(w, index, 0, rows)
        if side_of is None:
            return block_of(w, index, pl.multiple_of(grp * share, 16), pulled)
        return block_of(w, index, pl.multiple_of(side_of * pulled, 16), share)

    def z_copy(w, side, d, first=False):
        target = part_of(w, origin(side, d - 1), None)
        source = target
        if first:
            source = sources[w]
            if w != GATE and share:
                source = source.at[pl.ds(pl.multiple_of(grp * share, 16), pulled)]
        return pltpu.make_async_remote_copy(
            src_ref=source, dst_ref=target,
            send_sem=z_send.at[w, side, d - 1], recv_sem=z_recv.at[w, side, d - 1],
            device_id={"sp": sp + 1 if side == 0 else sp - 1}, device_id_type=MESH,
        )

    def z_arrival(w, side, d):
        place = part_of(w, origin(side, d), None)
        return pltpu.make_async_remote_copy(
            src_ref=place, dst_ref=place,
            send_sem=z_send.at[w, side, d - 1], recv_sem=z_recv.at[w, side, d - 1],
            device_id={"sp": sp + 1 if side == 0 else sp - 1}, device_id_type=MESH,
        )

    def y_copy(w, side, d, arriving=False):
        place = part_of(w, origin(side, d), 1 - grp if arriving else grp)
        return pltpu.make_async_remote_copy(
            src_ref=place, dst_ref=place,
            send_sem=y_send.at[w, side, d - 1], recv_sem=y_recv.at[w, side, d - 1],
            device_id={"grp": 1 - grp}, device_id_type=MESH,
        )

    def offer(w):
        for side in range(2):
            @pl.when(leaves(side, 1))
            def _(side=side):
                z_copy(w, side, 1, True).start()

    def relay_hop(w, d):
        for side in range(2):
            @pl.when(arrives(side, d))
            def _(side=side):
                z_arrival(w, side, d).wait_recv()

                @pl.when(leaves(side, d + 1))
                def _():
                    z_copy(w, side, d + 1).start()

                if share and w != GATE:
                    y_copy(w, side, d).start()

    def relay(w, low=1, high=None):
        if high is None:
            each(n_sp - low, lambda step: relay_hop(w, step + low))
        else:
            for d in range(low, min(high, n_sp - 1) + 1):
                relay_hop(w, d)

    def complete(w):
        own[w].wait()
        if share and w != GATE:
            def one(step):
                for side in range(2):
                    @pl.when(arrives(side, step + 1))
                    def _(side=side):
                        y_copy(w, side, step + 1, True).wait_recv()

            each(n_sp - 1, one)

    offer(KEY)
    offer(GATE)
    offer(VALUE)
    load_od.start()
    load_oc.start()

    load_tok.wait()
    chunk = 64
    for at in range(0, length, chunk):
        here = tok[at:at + chunk, :].astype(F32)
        scale = lax.rsqrt(jnp.mean(here * here, axis=-1, keepdims=True) + EPSILON)
        normed[at:at + chunk, :] = (here * scale * gain[...]).astype(BF16)

    def project(w):
        return jnp.dot(normed[...], targets[w][...], preferred_element_type=F32)

    def unit_rows(tensor):
        return tensor * lax.rsqrt(jnp.sum(tensor * tensor, axis=-1, keepdims=True) + EPSILON)

    def silu(tensor):
        return tensor * jax.nn.sigmoid(tensor)

    relay(GATE)
    relay(KEY)
    offer(QUERY)
    complete(GATE)
    gate_cols = jnp.zeros((length, 4 * heads), F32)
    gate_rows = jnp.zeros((4 * heads, length), F32)
    for index in range(n_sp):
        normed_part = normed[:, index * rows:(index + 1) * rows]
        gate_cols = gate_cols + lax.dot_general(normed_part, wg[index], NT, preferred_element_type=F32)
        gate_rows = gate_rows + lax.dot_general(wg[index], normed_part, NT, preferred_element_type=F32)

    row_at = lax.broadcasted_iota(jnp.int32, (length, length), 0)
    col_at = lax.broadcasted_iota(jnp.int32, (length, length), 1)

    complete(KEY)
    key_proj = silu(project(KEY))
    pairs = [(h, r) for h in range(heads) for r in range(2)]
    for h in range(heads):
        keys[h] = unit_rows(key_proj[:, h * head_width:(h + 1) * head_width])
    relay(VALUE, 1, 1)
    for h in range(heads):
        grams = bdot(keys[h], keys[h], NT)
        for r in range(2):
            p = 2 * h + r
            decay_col = ld[:, p:p + 1] * (0.5 + jax.nn.sigmoid(gate_cols[:, 2 * p:2 * p + 1]))
            decay_row = ldt[p:p + 1, :] * (0.5 + jax.nn.sigmoid(gate_rows[2 * p:2 * p + 1, :]))
            beta = jax.nn.sigmoid(gate_cols[:, 2 * p + 1:2 * p + 2] - BETA_SHIFT)
            if r == 0:
                seen_down, seen_across = row_at <= col_at, col_at <= row_at
            else:
                seen_down, seen_across = row_at >= col_at, col_at >= row_at
            cum_row = jnp.sum(jnp.where(seen_down, decay_col, 0.0), axis=0, keepdims=True)
            cum_col = jnp.sum(jnp.where(seen_across, decay_row, 0.0), axis=1, keepdims=True)
            weighting = jnp.where(
                seen_across, jnp.exp(jnp.where(seen_across, cum_col - cum_row, 0.0)), 0.0
            )
            gaps[p] = weighting
            betas[p] = jnp.broadcast_to(beta, (length, head_width))
            cums[p] = jnp.broadcast_to(cum_col, (length, head_width))
            lower = jnp.where(row_at != col_at, grams * weighting * beta, 0.0)
            rhs[p] = lower
            near = (row_at // 2 == col_at // 2)
            xinv[p] = jnp.where(row_at == col_at, 1.0, jnp.where(near, -lower, 0.0))

    size = 2
    while size < length:
        inside = (row_at // (2 * size) == col_at // (2 * size)) & (row_at // size != col_at // size)
        for p in range(len(pairs)):
            across = jnp.where(inside, rhs[p], 0.0)
            inverse = xinv[p]
            xinv[p] = inverse - bdot(inverse, bdot(across, inverse))
        if size == 2:
            relay(VALUE, 2)
            offer(GLU)
        if size == 32:
            relay(QUERY, 1, 1)
        if size == 128:
            relay(QUERY, 2, 2)
        size *= 2

    complete(VALUE)
    value_proj = silu(project(VALUE))
    eye = (
        lax.broadcasted_iota(jnp.int32, (head_width, head_width), 0)
        == lax.broadcasted_iota(jnp.int32, (head_width, head_width), 1)
    )
    for h, r in pairs:
        p = 2 * h + r
        beta, cum, key = betas[p], cums[p], keys[h]
        value = value_proj[:, h * head_width:(h + 1) * head_width]
        total = cum[length - 1:length, :] if r == 0 else cum[0:1, :]
        right = jnp.concatenate([beta * value, beta * key * jnp.exp(cum)], axis=1)
        solved = bdot(xinv[p], right)
        vals[p] = solved.astype(BF16)
        passed = bdot(key * jnp.exp(total - cum), solved, TN)
        ends[p] = passed[:, :head_width]
        maps[p] = (jnp.where(eye, jnp.exp(total), 0.0) - passed[:, head_width:]).astype(BF16)

    def place_of(r):
        return sp if r == 0 else n_sp - 1 - sp

    def chain_copy(r):
        dest = lax.rem(sp + 1, n_sp) if r == 0 else lax.rem(sp + n_sp - 1, n_sp)
        return pltpu.make_async_remote_copy(
            src_ref=chain_out.at[r], dst_ref=chain_in.at[r],
            send_sem=chain_send.at[r], recv_sem=chain_recv.at[r],
            device_id={"sp": dest}, device_id_type=MESH,
        )

    def chain_point(low, high):
        for r in range(2):
            at = place_of(r)

            @pl.when((at >= low) & (at <= high))
            def _(r=r, at=at):
                if low == 0:
                    for h in range(heads):
                        chain_in[r, h] = jnp.zeros((head_width, head_width), BF16)
                        chain_out[r, h] = ends[2 * h + r].astype(BF16)
                else:
                    chain_copy(r).wait_recv()
                    for h in range(heads):
                        p = 2 * h + r
                        chain_out[r, h] = (bdot(maps[p], chain_in[r, h]) + ends[p]).astype(BF16)

                @pl.when(at < n_sp - 1)
                def _():
                    chain_copy(r).start()

    chain_point(0, 0)
    relay(QUERY, 3)
    offer(OPEN)
    relay(GLU, 1, 1)
    complete(QUERY)
    query_proj = silu(project(QUERY))
    for h in range(heads):
        query = unit_rows(query_proj[:, h * head_width:(h + 1) * head_width]) * head_width ** -0.5
        scores = bdot(query, keys[h], NT)
        for r in range(2):
            p = 2 * h + r
            both = jnp.dot((scores * gaps[p]).astype(BF16), vals[p], preferred_element_type=F32)
            reads[p] = (query * jnp.exp(cums[p]) - both[:, head_width:]).astype(BF16)
            if r == 0:
                local_out[h] = both[:, :head_width]
            else:
                local_out[h] = local_out[h] + both[:, :head_width]
    chain_point(1, 1)
    relay(GLU, 2, 2)
    chain_point(2, 2)
    relay(GLU, 3)
    relay(OPEN, 1, 1)
    chain_point(3, n_sp - 1)
    complete(GLU)
    glu_proj = project(GLU)
    relay(OPEN, 2)
    complete(OPEN)
    gated = (glu_proj * jax.nn.sigmoid(project(OPEN))).astype(BF16)
    glu[...] = gated
    pad[HALO:HALO + length, :] = gated.astype(F32)

    def halo_copy(r):
        start = length - HALO if r == 0 else 0
        dest = lax.rem(sp + 1, n_sp) if r == 0 else lax.rem(sp + n_sp - 1, n_sp)
        return pltpu.make_async_remote_copy(
            src_ref=glu.at[pl.ds(start, HALO)], dst_ref=halo.at[r],
            send_sem=halo_send.at[r], recv_sem=halo_recv.at[r],
            device_id={"sp": dest}, device_id_type=MESH,
        )

    for r in range(2):
        @pl.when(place_of(r) < n_sp - 1)
        def _(r=r):
            halo_copy(r).start()
    for r in range(2):
        start = 0 if r == 0 else HALO + length

        @pl.when(place_of(r) > 0)
        def _(r=r, start=start):
            halo_copy(r).wait_recv()
            pad[start:start + HALO, :] = halo[r].astype(F32)

        @pl.when(place_of(r) == 0)
        def _(start=start):
            pad[start:start + HALO, :] = jnp.zeros((HALO, channels), F32)

    taps = ck.shape[0]
    for at in range(0, length, chunk):
        first = at + HALO - taps // 2
        total = pad[first:first + chunk, :] * ck[0:1, :]
        for j in range(1, taps):
            total = total + pad[first + j:first + j + chunk, :] * ck[j:j + 1, :]
        conv[at:at + chunk, :] = total
    filtered = conv[...]
    sum_col = jnp.sum(filtered, axis=-1, keepdims=True)
    square_col = jnp.sum(filtered * filtered, axis=-1, keepdims=True)
    same = row_at == col_at
    stat_out[...] = jnp.zeros(stat_out.shape, F32)
    stat_out[0:1, :] = jnp.sum(jnp.where(same, sum_col, 0.0), axis=0, keepdims=True)
    stat_out[1:2, :] = jnp.sum(jnp.where(same, square_col, 0.0), axis=0, keepdims=True)

    def stat_copy(step):
        return pltpu.make_async_remote_copy(
            src_ref=stat_out, dst_ref=stat_in.at[step],
            send_sem=stat_send.at[step], recv_sem=stat_recv.at[step],
            device_id={"tp": lax.rem(tp + step + 1, n_tp)}, device_id_type=MESH,
        )

    for step in range(n_tp - 1):
        stat_copy(step).start()

    joined_heads = []
    for h in range(heads):
        joined = local_out[h] + jnp.dot(reads[2 * h], chain_in[0, h], preferred_element_type=F32)
        joined = joined + jnp.dot(reads[2 * h + 1], chain_in[1, h], preferred_element_type=F32)
        scale = lax.rsqrt(jnp.mean(joined * joined, axis=-1, keepdims=True) + EPSILON)
        joined_heads.append((joined * scale * hgain[...]).astype(BF16))
    delta_mix = jnp.concatenate(joined_heads, axis=1) if heads > 1 else joined_heads[0]
    load_od.wait()
    load_oc.wait()
    columns = width // n_tp
    for dest in range(n_tp):
        at = slice(dest * columns, (dest + 1) * columns)
        conv_acc[dest] = lax.dot_general(delta_mix, od[at, :], NT, preferred_element_type=F32)

    stats = stat_out[0:2, :]
    for step in range(n_tp - 1):
        stat_copy(step).wait_recv()
        stats = stats + stat_in[step, 0:2, :]
    center = jnp.sum(jnp.where(same, stats[0:1, :], 0.0), axis=1, keepdims=True) / conv_total
    squares = jnp.sum(jnp.where(same, stats[1:2, :], 0.0), axis=1, keepdims=True) / conv_total
    spread = squares - center * center
    normal = (filtered - center) * lax.rsqrt(spread + EPSILON)
    conv_mix = silu(normal * ng[...] + ns[...]).astype(BF16)

    chip, core = tp // 2, lax.rem(tp, 2)
    chips = n_tp // 2
    sibling = chip * 2 + 1 - core

    def there(p, place):
        return lax.rem(chip + p, chips) * 2 + place

    def term_of(dest):
        at = pl.ds(pl.multiple_of(dest * columns, 16), columns)
        return conv_acc[dest] + lax.dot_general(conv_mix, oc[at, :], NT, preferred_element_type=F32)

    def pair_copy(p):
        return pltpu.make_async_remote_copy(
            src_ref=pair_out.at[p], dst_ref=pair_in.at[p],
            send_sem=pair_send.at[p], recv_sem=pair_recv.at[p],
            device_id={"tp": sibling}, device_id_type=MESH,
        )

    def part_copy(p):
        return pltpu.make_async_remote_copy(
            src_ref=part_out.at[p - 1], dst_ref=part_in.at[p - 1],
            send_sem=part_send.at[p - 1], recv_sem=part_recv.at[p - 1],
            device_id={"tp": there(p, core)}, device_id_type=MESH,
        )

    slots = list(range(1, chips)) + [0]
    for p in slots:
        pair_out[p] = term_of(there(p, 1 - core)).astype(BF16)
        pair_copy(p).start()
    for p in slots:
        term = term_of(there(p, core))
        pair_copy(p).wait_recv()
        term = term + pair_in[p].astype(F32)
        if p:
            part_out[p - 1] = term.astype(BF16)
            part_copy(p).start()
        else:
            result = term
    for p in range(1, chips):
        part_copy(p).wait_recv()
        result = result + part_in[p - 1].astype(F32)
    out[...] = result.astype(BF16)

    for w in range(6):
        def one(step, w=w):
            for side in range(2):
                @pl.when(leaves(side, step + 1))
                def _(side=side):
                    z_copy(w, side, step + 1).wait_send()

                if share and w != GATE:
                    @pl.when(arrives(side, step + 1))
                    def _(side=side):
                        y_copy(w, side, step + 1).wait_send()

        each(n_sp - 1, one)
    for r in range(2):
        @pl.when(place_of(r) < n_sp - 1)
        def _(r=r):
            chain_copy(r).wait_send()
            halo_copy(r).wait_send()
    for step in range(n_tp - 1):
        stat_copy(step).wait_send()
    for p in range(chips):
        pair_copy(p).wait_send()
        if p:
            part_copy(p).wait_send()


def solution(mesh):
    n_grp, n_sp, n_tp = mesh.shape["grp"], mesh.shape["sp"], mesh.shape["tp"]

    def on_device(tokens_in, input_gain, w_query, w_key, w_value, w_gates, w_glu_value,
                  sigmoid_opener_matrix, log_decay, head_gain, conv_kernel, norm_gain, norm_shift,
                  out_delta, out_conv):
        length, width = tokens_in.shape
        head_width = head_gain.shape[0]
        head_cols = w_query.shape[1]
        heads = head_cols // head_width
        channels = w_glu_value.shape[1]
        rows = w_query.shape[0]
        pairs = 2 * heads
        columns = width // n_tp
        dma, vmem = pltpu.SemaphoreType.DMA, pltpu.VMEM
        anywhere = pl.BlockSpec(memory_space=pltpu.HBM)
        inside = pl.BlockSpec(memory_space=pltpu.VMEM)
        scratch = [
            vmem((length, width), BF16), vmem((length, width), BF16),
            vmem((width, head_cols), BF16), vmem((n_sp, 4 * heads, rows), BF16),
            vmem((width, head_cols), BF16), vmem((width, head_cols), BF16),
            vmem((width, channels), BF16), vmem((width, channels), BF16),
            vmem((width, head_cols), BF16), vmem((width, channels), BF16),
            vmem((heads, length, head_width), F32), vmem((pairs, length, 2 * head_width), BF16),
            vmem((pairs, length, head_width), F32), vmem((pairs, length, head_width), F32),
            vmem((pairs, length, length), F32), vmem((pairs, length, length), F32),
            vmem((pairs, length, length), F32),
            vmem((heads, length, head_width), F32), vmem((pairs, length, head_width), BF16),
            vmem((pairs, head_width, head_width), BF16), vmem((pairs, head_width, head_width), F32),
            vmem((2, heads, head_width, head_width), BF16), vmem((2, heads, head_width, head_width), BF16),
            vmem((length, channels), BF16), vmem((2, HALO, channels), BF16),
            vmem((length + 2 * HALO, channels), F32), vmem((length, channels), F32),
            vmem((8, length), F32), vmem((n_tp - 1, 8, length), F32),
            vmem((n_tp, length, columns), F32),
            vmem((n_tp // 2, length, columns), BF16), vmem((n_tp // 2, length, columns), BF16),
            vmem((n_tp // 2, length, columns), BF16), vmem((n_tp // 2, length, columns), BF16),
            dma((9,)),
            dma((6, 2, n_sp - 1)), dma((6, 2, n_sp - 1)),
            dma((6, 2, n_sp - 1)), dma((6, 2, n_sp - 1)),
            dma((2,)), dma((2,)), dma((2,)), dma((2,)),
            dma((n_tp - 1,)), dma((n_tp - 1,)), dma((n_tp // 2,)), dma((n_tp // 2,)),
            dma((n_tp // 2,)), dma((n_tp // 2,)),
        ]
        return pl.pallas_call(
            functools.partial(kernel, (n_grp, n_sp, n_tp, float(channels * n_tp))),
            out_shape=jax.ShapeDtypeStruct((length, columns), BF16),
            in_specs=[anywhere, inside] + [anywhere] * 6 + [inside] * 6 + [anywhere] * 2,
            out_specs=inside,
            scratch_shapes=scratch,
            compiler_params=pltpu.CompilerParams(
                collective_id=0, has_side_effects=True, vmem_limit_bytes=60 * 1024 * 1024
            ),
        )(
            tokens_in, input_gain.reshape(1, width), w_key, w_gates.T, w_value, w_query,
            w_glu_value, sigmoid_opener_matrix, log_decay, log_decay.T,
            head_gain.reshape(1, head_width), conv_kernel, norm_gain.reshape(1, channels),
            norm_shift.reshape(1, channels), out_delta, out_conv,
        )

    placed = (
        P(("grp", "sp"), None), P(), P("sp", "tp"), P("sp", "tp"), P("sp", "tp"), P("sp", "tp"),
        P("sp", "tp"), P("sp", "tp"), P(("grp", "sp"), "tp"), P(), P(None, "tp"), P("tp"), P("tp"),
        P(None, "tp"), P(None, "tp"),
    )
    return jax.shard_map(
        on_device, mesh=mesh, in_specs=placed, out_specs=P(("grp", "sp"), "tp"), check_vma=False
    )
```

profile of v0, /device:TPU:0, one launch (start us, length us, event | category | flops | bytes accessed | tf_op | source)
XLA Modules:
  0.0 82.9 jit_solution(13828135732529340831)
XLA Ops:
  0.0 0.0 copy-start
  0.0 0.7 copy-done
  0.7 0.8 copy.16.ld
  1.5 79.7 %shard_map.145 = bf16[256,512]{1,0:T(8,128)(2,1)} custom-call(bf16[256,2048]{1,0:T(8,128)(2,1)} %tok_h.1, f32[1,2048]{1,0:T(1,128)} %bitcast.7, bf16[512,256]{1,0:T(8,128)(2,1)} %wk_h.1, bf16[8,512]{1,0:T(8,128)(2,1)} %bitcast.8, bf16[512,256]{1,0:T(8,128)(2,1)} %wv_h.1, bf16[512,256]{1,0:T(8,128)(2,1)} %wq_h.1, bf16[512,256]{1,0:T(8,128)(2,1)} %wa_h.1, ...), custom_call_target="tpu_custom_call" | custom-call | tf_op jit(solution)/shard_map/pallas_call | solution.py:525
  81.2 1.7 %copy.18 = bf16[256,512]{1,0:T(8,128)(2,1)} copy(bf16[256,512]{1,0:T(8,128)(2,1)} %shard_map.145) | data formatting | bytes 524288
Async XLA Ops:
  0.0 0.7 copy-start
where the time goes:
time: 84.4 us; the launch traced here: 82.9 us
  Pallas kernels  79.7 us (94%)
  local copies, waits for them, and re-layouts  3.16 us (4%)
    pallas_call x1, Pallas kernels, on_device(): pl.pallas_call(functools.partial(kernel, (n_grp, n_sp, n_tp, float(channe...  79.7 us
    unnamed x4, local copies, waits for them, and re-layouts  3.16 us

commit v1 on v0

--- a/solution.py
+++ b/solution.py
@@ -479,6 +479,666 @@
             part_copy(p).wait_send()
 
 
+def fused(cfg, tok_h, gain, wk_h, wg_h, wv_h, wq_h, wa_h, wb_h, ldt, hgain, ck, ng, ns, od_h, oc_h,
+          out,
+          tok, nt, wk, wv, wq, wab, wg, odg, ocg, ldo,
+          keys, vals, betas, cums, xinv, gaps, rhs, local_out, reads, maps, ends,
+          chain_in, chain_out, gout, gend, main_in, edge_in, pad, conv, stat_out, stat_in,
+          dall, dm_out, call,
+          local_sem, z_send, z_recv, ty_send, ty_recv, tf_send, tf_recv, tz_send, tz_recv,
+          ld_send, ld_recv, od_send, od_recv, chain_send, chain_recv,
+          main_send, main_recv, edge_send, edge_recv, far_send, rim_send,
+          stat_send, stat_recv, dg_send, dg_recv, df_send, df_recv, cg_send, cg_recv, cf_send, cf_recv):
+    n_sp, n_tp, conv_total = cfg
+    grp, sp, tp = lax.axis_index("grp"), lax.axis_index("sp"), lax.axis_index("tp")
+    length, width = tok.shape
+    rows = wk_h.shape[0]
+    head_width = hgain.shape[1]
+    cols = wk.shape[1]
+    heads = cols // head_width
+    channels = wab.shape[1] // 2
+    columns = out.shape[1]
+    units = [(j, h) for j in range(2) for h in range(heads)]
+    n_units = len(units)
+    pairs = [(u, r) for u in range(n_units) for r in range(2)]
+    chip, core = tp // 2, lax.rem(tp, 2)
+    chips = n_tp // 2
+    sibling = tp + 1 - 2 * core
+    other = 1 - grp
+    edge = (sp == 0) | (sp == n_sp - 1)
+    inner = (sp > 0) & (sp < n_sp - 1)
+    helps = (sp == 1) | (sp == n_sp - 2)
+    helper = jnp.where(sp == 0, 1, n_sp - 2)
+    helped = jnp.where(sp == 1, 0, n_sp - 1)
+    sources = (wk_h, wg_h, wv_h, wq_h, wa_h, wb_h)
+    plain = {KEY: wk, VALUE: wv, QUERY: wq}
+
+    def remote(src, dst, send, recv, **where):
+        return pltpu.make_async_remote_copy(
+            src_ref=src, dst_ref=dst, send_sem=send, recv_sem=recv, device_id=where, device_id_type=MESH
+        )
+
+    def source(w):
+        if w == GATE:
+            return wg_h
+        size = channels if w in (GLU, OPEN) else cols
+        return sources[w].at[:, pl.ds(pl.multiple_of(grp * size, 128), size)]
+
+    def target(w, index):
+        if w == GATE:
+            return wg.at[index]
+        at = pl.ds(pl.multiple_of(index * rows, 16), rows)
+        if w in (GLU, OPEN):
+            return wab.at[at, pl.ds(channels if w == OPEN else 0, channels)]
+        return plain[w].at[at]
+
+    load_tok = pltpu.make_async_copy(tok_h, tok, local_sem.at[0])
+    load_tok.start()
+    own = [pltpu.make_async_copy(source(w), target(w, sp), local_sem.at[1 + w]) for w in range(6)]
+    for w in (KEY, GATE, VALUE, QUERY):
+        own[w].start()
+
+    @pl.when(inner)
+    def _():
+        own[GLU].start()
+        own[OPEN].start()
+
+    def od_rows(index):
+        return pl.ds(pl.multiple_of(index * columns, 16), columns)
+
+    load_od = pltpu.make_async_copy(od_h.at[od_rows(tp)], odg.at[tp], local_sem.at[7])
+    load_oc = pltpu.make_async_copy(oc_h.at[od_rows(tp)], ocg.at[tp], local_sem.at[8])
+    load_od.start()
+    load_oc.start()
+
+    barrier = pltpu.get_barrier_semaphore()
+
+    def greet(**where):
+        pl.semaphore_signal(barrier, inc=1, device_id=where, device_id_type=MESH)
+
+    for step in range(n_tp - 1):
+        peer = lax.rem(tp + step + 1, n_tp)
+        greet(tp=peer)
+        greet(tp=peer, grp=other)
+    greet(grp=other)
+
+    @pl.when(sp > 0)
+    def _():
+        greet(sp=sp - 1)
+        greet(sp=sp - 1, grp=other)
+
+    @pl.when(sp < n_sp - 1)
+    def _():
+        greet(sp=sp + 1)
+        greet(sp=sp + 1, grp=other)
+
+    load_tok.wait()
+    chunk = 64
+    for at in range(0, length, chunk):
+        here = tok[at:at + chunk, :].astype(F32)
+        scale = lax.rsqrt(jnp.mean(here * here, axis=-1, keepdims=True) + EPSILON)
+        nt[at:at + chunk, :] = (here * scale * gain[...]).astype(BF16)
+
+    @pl.when(edge)
+    def _():
+        pl.semaphore_wait(barrier, 2 * n_tp + 1)
+
+    @pl.when(inner)
+    def _():
+        pl.semaphore_wait(barrier, 2 * n_tp + 3)
+
+    def wide(w):
+        return 1 if w in (GLU, OPEN) else 0
+
+    def arrives(w, side, d):
+        ok = (sp - d >= 0) if side == 0 else (sp + d < n_sp)
+        return ok & inner if wide(w) else ok
+
+    def leaves(w, side, d):
+        if side == 0:
+            return (sp - (d - 1) >= 0) & (sp < n_sp - 1 - wide(w))
+        return (sp + (d - 1) < n_sp) & (sp > wide(w))
+
+    def z_copy(w, side, d):
+        back = d - 1
+        place = target(w, sp - back if side == 0 else sp + back)
+        return remote(
+            source(w) if d == 1 else place, place, z_send.at[w, side, d - 1], z_recv.at[w, side, d - 1],
+            sp=sp + 1 if side == 0 else sp - 1,
+        )
+
+    def z_arrival(w, side, d):
+        place = target(w, sp - d if side == 0 else sp + d)
+        return remote(
+            place, place, z_send.at[w, side, d - 1], z_recv.at[w, side, d - 1],
+            sp=sp + 1 if side == 0 else sp - 1,
+        )
+
+    def offer(w, where):
+        for side in range(2):
+            @pl.when(leaves(w, side, 1) & where)
+            def _(side=side):
+                z_copy(w, side, 1).start()
+
+    def relay(w, d):
+        if d > n_sp - 1:
+            return
+        for side in range(2):
+            @pl.when(arrives(w, side, d))
+            def _(side=side):
+                z_arrival(w, side, d).wait_recv()
+                if d < n_sp - 1:
+                    @pl.when(leaves(w, side, d + 1))
+                    def _():
+                        z_copy(w, side, d + 1).start()
+
+    pieces = ty_send.shape[1]
+    half = length // 2
+    piece = half // pieces
+
+    def part(block, side, c):
+        return nt.at[pl.ds(pl.multiple_of(block * length + side * half + c * piece, 16), piece)]
+
+    def tok_y(k, c):
+        return remote(part(2 * k, core, c), part(2 * k + 1, core, c), ty_send.at[k, c], ty_recv.at[k, c], grp=other)
+
+    def tok_z(c):
+        return remote(part(0, core, c), part(2, core, c), tz_send.at[c], tz_recv.at[c], sp=helper)
+
+    def tok_f(block, c):
+        return remote(
+            part(block, core, c), part(block, core, c), tf_send.at[block - 1, c], tf_recv.at[block - 1, c], tp=sibling
+        )
+
+    def tok_f_arrival(block, c):
+        place = part(block, 1 - core, c)
+        return remote(place, place, tf_send.at[block - 1, c], tf_recv.at[block - 1, c], tp=sibling)
+
+    def pass_y(k, c):
+        tok_y(k, c).wait_recv()
+        tok_f(2 * k + 1, c).start()
+
+    def pass_z(c):
+        @pl.when(helps)
+        def _():
+            tok_z(c).wait_recv()
+            tok_y(1, c).start()
+            tok_f(2, c).start()
+
+    def pass_far(c):
+        @pl.when(helps)
+        def _():
+            pass_y(1, c)
+
+    ld_copy = remote(ldt, ldo, ld_send.at[0], ld_recv.at[0], grp=other)
+
+    def od_copy(m, step):
+        dest = lax.rem(tp + step + 1, n_tp)
+        src, dst = ((od_h, odg), (oc_h, ocg))[m]
+        return remote(src.at[od_rows(dest)], dst.at[tp], od_send.at[m, step], od_recv.at[m, step], tp=dest)
+
+    def od_arrival(m, step):
+        origin = lax.rem(tp + n_tp - step - 1, n_tp)
+        place = (odg, ocg)[m].at[origin]
+        return remote(place, place, od_send.at[m, step], od_recv.at[m, step], tp=origin)
+
+    everywhere = sp >= 0
+    offer(GATE, everywhere)
+    offer(KEY, everywhere)
+    for c in range(pieces):
+        tok_y(0, c).start()
+    ld_copy.start()
+    offer(VALUE, everywhere)
+    offer(GLU, edge)
+
+    @pl.when(edge)
+    def _():
+        for c in range(pieces):
+            tok_z(c).start()
+
+    offer(OPEN, edge)
+    offer(QUERY, edge)
+    for m in (1, 0):
+        for step in range(n_tp - 1):
+            od_copy(m, step).start()
+
+    def dot(a, b, dims=NN):
+        return lax.dot_general(a, b, dims, preferred_element_type=F32)
+
+    def unit_rows(tensor):
+        return tensor * lax.rsqrt(jnp.sum(tensor * tensor, axis=-1, keepdims=True) + EPSILON)
+
+    def silu(tensor):
+        return tensor * jax.nn.sigmoid(tensor)
+
+    relay(GATE, 1)
+    relay(KEY, 1)
+    relay(GATE, 2)
+    relay(KEY, 2)
+    relay(VALUE, 1)
+    offer(GLU, inner)
+    for d in range(3, n_sp):
+        relay(GATE, d)
+        relay(KEY, d)
+    relay(GLU, 1)
+    offer(OPEN, inner)
+    offer(QUERY, inner)
+    for c in range(pieces):
+        pass_y(0, c)
+    pass_z(0)
+    own[GATE].wait()
+    own[KEY].wait()
+    ld_copy.wait_recv()
+    for c in range(pieces):
+        tok_f_arrival(1, c).wait_recv()
+
+    both = 2 * length
+    gate_cols = jnp.zeros((both, wg.shape[1]), F32)
+    gate_rows = jnp.zeros((wg.shape[1], both), F32)
+    for index in range(n_sp):
+        normed_part = nt[0:both, index * rows:(index + 1) * rows]
+        gate_cols = gate_cols + dot(normed_part, wg[index], NT)
+        gate_rows = gate_rows + dot(wg[index], normed_part, NT)
+    mine = grp == 0
+    gates = 4 * heads
+    gate_cols = jnp.where(mine, gate_cols[:, :gates], gate_cols[:, gates:])
+    gate_rows = jnp.where(mine, gate_rows[:gates, :], gate_rows[gates:, :])
+    rates = [
+        jnp.where(mine, log[:2 * heads, :], log[2 * heads:, :]) for log in (ldt[...], ldo[...])
+    ]
+
+    row_at = lax.broadcasted_iota(jnp.int32, (length, length), 0)
+    col_at = lax.broadcasted_iota(jnp.int32, (length, length), 1)
+    same = row_at == col_at
+
+    key_proj = silu(dot(nt[0:both, :], wk[...]))
+    pass_z(1)
+    relay(VALUE, 2)
+    for u, (j, h) in enumerate(units):
+        keys[u] = unit_rows(key_proj[j * length:(j + 1) * length, h * head_width:(h + 1) * head_width])
+    for u, (j, h) in enumerate(units):
+        grams = bdot(keys[u], keys[u], NT)
+        for r in range(2):
+            p = 2 * u + r
+            g = 4 * h + 2 * r
+            span = slice(j * length, (j + 1) * length)
+            decay_row = rates[j][2 * h + r:2 * h + r + 1, :] * (0.5 + jax.nn.sigmoid(gate_rows[g:g + 1, span]))
+            beta = jax.nn.sigmoid(gate_cols[span, g + 1:g + 2] - BETA_SHIFT)
+            seen = col_at <= row_at if r == 0 else col_at >= row_at
+            cum_col = jnp.sum(jnp.where(seen, decay_row, 0.0), axis=1, keepdims=True)
+            cum_row = jnp.sum(jnp.where(same, cum_col, 0.0), axis=0, keepdims=True)
+            weighting = jnp.where(seen, jnp.exp(jnp.where(seen, cum_col - cum_row, 0.0)), 0.0)
+            gaps[p] = weighting
+            betas[p] = jnp.broadcast_to(beta, (length, head_width))
+            cums[p] = jnp.broadcast_to(cum_col, (length, head_width))
+            lower = jnp.where(same, 0.0, grams * weighting * beta)
+            rhs[p] = lower
+            near = (row_at // 2 == col_at // 2)
+            xinv[p] = jnp.where(same, 1.0, jnp.where(near, -lower, 0.0))
+
+    service = {
+        2: [lambda: pass_z(2), lambda: pass_far(0)],
+        8: [lambda: pass_z(3), lambda: pass_far(1)],
+        32: [lambda: pass_far(2)],
+        64: [lambda: relay(GLU, 2)],
+        128: [lambda: pass_far(3), lambda: relay(OPEN, 1)],
+    }
+    size = 2
+    while size < length:
+        inside = (row_at // (2 * size) == col_at // (2 * size)) & (row_at // size != col_at // size)
+        for p in range(len(pairs)):
+            across = jnp.where(inside, rhs[p], 0.0)
+            inverse = xinv[p]
+            xinv[p] = inverse - bdot(inverse, bdot(across, inverse))
+        for act in service.get(size, ()):
+            act()
+        size *= 2
+
+    own[VALUE].wait()
+    for d in range(3, n_sp):
+        relay(VALUE, d)
+    value_proj = silu(dot(nt[0:both, :], wv[...]))
+    eye = (
+        lax.broadcasted_iota(jnp.int32, (head_width, head_width), 0)
+        == lax.broadcasted_iota(jnp.int32, (head_width, head_width), 1)
+    )
+    for u, r in pairs:
+        p = 2 * u + r
+        j, h = units[u]
+        beta, cum, key = betas[p], cums[p], keys[u]
+        value = value_proj[j * length:(j + 1) * length, h * head_width:(h + 1) * head_width]
+        total = cum[length - 1:length, :] if r == 0 else cum[0:1, :]
+        right = jnp.concatenate([beta * value, beta * key * jnp.exp(cum)], axis=1)
+        solved = bdot(xinv[p], right)
+        vals[p] = solved.astype(BF16)
+        passed = bdot(key * jnp.exp(total - cum), solved, TN)
+        ends[p] = passed[:, :head_width]
+        maps[p] = (jnp.where(eye, jnp.exp(total), 0.0) - passed[:, head_width:]).astype(BF16)
+
+    def place_of(r):
+        return sp if r == 0 else n_sp - 1 - sp
+
+    def chain_copy(r):
+        dest = sp + 1 if r == 0 else sp - 1
+        return remote(chain_out.at[r], chain_in.at[r], chain_send.at[r], chain_recv.at[r], sp=dest)
+
+    def chain_point(low, high):
+        for r in range(2):
+            at = place_of(r)
+
+            @pl.when((at >= low) & (at <= high))
+            def _(r=r, at=at):
+                if low == 0:
+                    for u in range(n_units):
+                        chain_in[r, u] = jnp.zeros((head_width, head_width), BF16)
+                        chain_out[r, u] = ends[2 * u + r].astype(BF16)
+                else:
+                    chain_copy(r).wait_recv()
+                    for u in range(n_units):
+                        p = 2 * u + r
+                        chain_out[r, u] = (bdot(maps[p], chain_in[r, u]) + ends[p]).astype(BF16)
+
+                @pl.when(at < n_sp - 1)
+                def _():
+                    chain_copy(r).start()
+
+    chain_point(0, 0)
+    for d in range(3, n_sp):
+        relay(GLU, d)
+    relay(QUERY, 1)
+    relay(OPEN, 2)
+    for d in range(3, n_sp):
+        relay(OPEN, d)
+
+    def gated(first, count):
+        x = dot(nt[first * length:(first + count) * length, :], wab[...])
+        return (x[:, :channels] * jax.nn.sigmoid(x[:, channels:])).astype(BF16)
+
+    def owner(j):
+        return grp if j == 0 else other
+
+    def main_y():
+        return remote(gout, main_in.at[grp], main_send.at[0], main_recv.at[grp], grp=other)
+
+    def main_arrival(h):
+        return remote(main_in.at[h], main_in.at[h], main_send.at[0], main_recv.at[h], grp=other)
+
+    def far_copy(j):
+        return remote(gend.at[j], main_in.at[grp], far_send.at[j], main_recv.at[grp], sp=helped, grp=owner(j))
+
+    def edge_copy(side, j):
+        start = length - HALO if side == 0 else 0
+        src = main_in.at[grp, pl.ds(start, HALO)] if j == 0 else gout.at[pl.ds(start, HALO)]
+        return remote(
+            src, edge_in.at[side, grp], edge_send.at[side, j], edge_recv.at[side, grp],
+            sp=sp + 1 if side == 0 else sp - 1, grp=owner(j),
+        )
+
+    def rim_copy(side):
+        start = length - HALO if side == 0 else 0
+        return remote(
+            gend.at[1, pl.ds(start, HALO)], edge_in.at[side, grp], rim_send.at[side], edge_recv.at[side, grp], grp=other
+        )
+
+    def edge_arrival(side, h):
+        place = edge_in.at[side, h]
+        return remote(place, place, edge_send.at[side, 0], edge_recv.at[side, h], grp=other)
+
+    @pl.when(inner)
+    def _():
+        own[GLU].wait()
+        own[OPEN].wait()
+
+        @pl.when(helps)
+        def _():
+            for c in range(pieces):
+                tok_f_arrival(2, c).wait_recv()
+                tok_f_arrival(3, c).wait_recv()
+            far = gated(2, 2)
+            gend[0] = far[:length]
+            gend[1] = far[length:]
+            for j in range(2):
+                far_copy(j).start()
+            for side, at in ((0, 1), (1, n_sp - 2)):
+                @pl.when(sp == at)
+                def _(side=side):
+                    rim_copy(side).start()
+                    start = length - HALO if side == 0 else 0
+                    edge_in[side, grp] = gend[0, start:start + HALO, :]
+
+        near = gated(0, 2)
+        main_in[grp] = near[:length]
+        gout[...] = near[length:]
+        main_y().start()
+        for side in range(2):
+            for j in range(2):
+                edge_copy(side, j).start()
+
+    chain_point(1, 1)
+    relay(QUERY, 2)
+    for at in range(2, n_sp - 1):
+        chain_point(at, at)
+        relay(QUERY, at + 1)
+    chain_point(n_sp - 1, n_sp - 1)
+
+    for h in range(2):
+        @pl.when(~(inner & (grp == h)))
+        def _(h=h):
+            main_arrival(h).wait_recv()
+
+        @pl.when((sp > 0) & ~((sp == 1) & (grp == h)))
+        def _(h=h):
+            edge_arrival(0, h).wait_recv()
+
+        @pl.when((sp < n_sp - 1) & ~((sp == n_sp - 2) & (grp == h)))
+        def _(h=h):
+            edge_arrival(1, h).wait_recv()
+
+        pad[h, HALO:HALO + length, :] = main_in[h].astype(F32)
+        for side, start, none in ((0, 0, 0), (1, HALO + length, n_sp - 1)):
+            @pl.when(sp != none)
+            def _(h=h, side=side, start=start):
+                pad[h, start:start + HALO, :] = edge_in[side, h].astype(F32)
+
+            @pl.when(sp == none)
+            def _(h=h, start=start):
+                pad[h, start:start + HALO, :] = jnp.zeros((HALO, channels), F32)
+
+    taps = ck.shape[0]
+    for h in range(2):
+        lanes = slice(h * channels, (h + 1) * channels)
+        for at in range(0, length, chunk):
+            first = at + HALO - taps // 2
+            total = pad[h, first:first + chunk, :] * ck[0:1, lanes]
+            for k in range(1, taps):
+                total = total + pad[h, first + k:first + k + chunk, :] * ck[k:k + 1, lanes]
+            conv[at:at + chunk, lanes] = total
+    filtered = conv[...]
+    sum_col = jnp.sum(filtered, axis=-1, keepdims=True)
+    square_col = jnp.sum(filtered * filtered, axis=-1, keepdims=True)
+    stat_out[...] = jnp.zeros(stat_out.shape, F32)
+    stat_out[0:1, :] = jnp.sum(jnp.where(same, sum_col, 0.0), axis=0, keepdims=True)
+    stat_out[1:2, :] = jnp.sum(jnp.where(same, square_col, 0.0), axis=0, keepdims=True)
+
+    def stat_copy(step):
+        return remote(
+            stat_out, stat_in.at[step], stat_send.at[step], stat_recv.at[step], tp=lax.rem(tp + step + 1, n_tp)
+        )
+
+    for step in range(n_tp - 1):
+        stat_copy(step).start()
+
+    own[QUERY].wait()
+    query_proj = silu(dot(nt[0:both, :], wq[...]))
+    for u, (j, h) in enumerate(units):
+        query = query_proj[j * length:(j + 1) * length, h * head_width:(h + 1) * head_width]
+        query = unit_rows(query) * head_width ** -0.5
+        scores = bdot(query, keys[u], NT)
+        for r in range(2):
+            p = 2 * u + r
+            pair = dot((scores * gaps[p]).astype(BF16), vals[p])
+            reads[p] = (query * jnp.exp(cums[p]) - pair[:, head_width:]).astype(BF16)
+            if r == 0:
+                local_out[u] = pair[:, :head_width]
+            else:
+                local_out[u] = local_out[u] + pair[:, :head_width]
+
+    def mixed_head(u):
+        joined = local_out[u] + dot(reads[2 * u], chain_in[0, u]) + dot(reads[2 * u + 1], chain_in[1, u])
+        scale = lax.rsqrt(jnp.mean(joined * joined, axis=-1, keepdims=True) + EPSILON)
+        return (joined * scale * hgain[...]).astype(BF16)
+
+    def chip_at(q):
+        return lax.rem(chip + q, chips)
+
+    def chip_back(q):
+        return lax.rem(chip + chips - q, chips)
+
+    def dg_copy(a, q):
+        src = dall.at[tp, grp] if a == 0 else dm_out
+        where = {"tp": chip_at(q) * 2 + core}
+        if a:
+            where["grp"] = other
+        return remote(src, dall.at[tp, grp], dg_send.at[a, q], dg_recv.at[a, q], **where)
+
+    def d_block(a, q, side):
+        return dall.at[chip_back(q) * 2 + side, other if a else grp]
+
+    def dg_arrival(a, q):
+        place = d_block(a, q, core)
+        return remote(place, place, dg_send.at[a, q], dg_recv.at[a, q], tp=sibling)
+
+    def df_copy(a, q, arriving=False):
+        place = d_block(a, q, 1 - core if arriving else core)
+        return remote(place, place, df_send.at[a, q], df_recv.at[a, q], tp=sibling)
+
+    def cg_copy(q):
+        return remote(call.at[tp], call.at[tp], cg_send.at[q], cg_recv.at[q], tp=chip_at(q) * 2 + core)
+
+    def cg_arrival(q):
+        place = call.at[chip_back(q) * 2 + core]
+        return remote(place, place, cg_send.at[q], cg_recv.at[q], tp=sibling)
+
+    def cf_copy(q, arriving=False):
+        place = call.at[chip_back(q) * 2 + (1 - core if arriving else core)]
+        return remote(place, place, cf_send.at[q], cf_recv.at[q], tp=sibling)
+
+    direct = [(a, q) for q in range(chips) for a in (1, 0) if (a, q) != (0, 0)]
+
+    for h in range(heads):
+        dm_out[:, h * head_width:(h + 1) * head_width] = mixed_head(heads + h)
+    for q in range(chips - 1, -1, -1):
+        dg_copy(1, q).start()
+    for h in range(heads):
+        dall[tp, grp, :, h * head_width:(h + 1) * head_width] = mixed_head(h)
+    for q in range(1, chips):
+        dg_copy(0, q).start()
+    df_copy(0, 0).start()
+
+    stats = stat_out[0:2, :]
+    for step in range(n_tp - 1):
+        stat_copy(step).wait_recv()
+        stats = stats + stat_in[step, 0:2, :]
+    center = jnp.sum(jnp.where(same, stats[0:1, :], 0.0), axis=1, keepdims=True) / conv_total
+    squares = jnp.sum(jnp.where(same, stats[1:2, :], 0.0), axis=1, keepdims=True) / conv_total
+    spread = squares - center * center
+    normal = (conv[...] - center) * lax.rsqrt(spread + EPSILON)
+    call[tp] = silu(normal * ng[...] + ns[...]).astype(BF16)
+    for q in range(1, chips):
+        cg_copy(q).start()
+    cf_copy(0).start()
+
+    for m in range(2):
+        for step in range(n_tp - 1):
+            od_arrival(m, step).wait_recv()
+    load_od.wait()
+    load_oc.wait()
+
+    for a, q in direct:
+        dg_arrival(a, q).wait_recv()
+        df_copy(a, q).start()
+    for q in range(1, chips):
+        cg_arrival(q).wait_recv()
+        cf_copy(q).start()
+
+    def delta_term(t):
+        return dot(jnp.concatenate([dall[t, 0], dall[t, 1]], axis=1), odg[t], NT)
+
+    def conv_term(t):
+        return dot(call[t], ocg[t], NT)
+
+    result = delta_term(tp)
+    for q in range(chips):
+        t = chip_back(q) * 2 + core
+        if q:
+            result = result + delta_term(t)
+        result = result + conv_term(t)
+    for q in range(chips):
+        t = chip_back(q) * 2 + 1 - core
+        df_copy(0, q, True).wait_recv()
+        df_copy(1, q, True).wait_recv()
+        result = result + delta_term(t)
+    for q in range(chips):
+        t = chip_back(q) * 2 + 1 - core
+        cf_copy(q, True).wait_recv()
+        result = result + conv_term(t)
+    out[...] = result.astype(BF16)
+
+    for w in range(6):
+        for d in range(1, n_sp):
+            for side in range(2):
+                @pl.when(leaves(w, side, d))
+                def _(w=w, d=d, side=side):
+                    z_copy(w, side, d).wait_send()
+    for c in range(pieces):
+        tok_y(0, c).wait_send()
+        tok_f(1, c).wait_send()
+
+        @pl.when(edge)
+        def _(c=c):
+            tok_z(c).wait_send()
+
+        @pl.when(helps)
+        def _(c=c):
+            tok_y(1, c).wait_send()
+            tok_f(2, c).wait_send()
+            tok_f(3, c).wait_send()
+    ld_copy.wait_send()
+    for m in range(2):
+        for step in range(n_tp - 1):
+            od_copy(m, step).wait_send()
+    for r in range(2):
+        @pl.when(place_of(r) < n_sp - 1)
+        def _(r=r):
+            chain_copy(r).wait_send()
+
+    @pl.when(inner)
+    def _():
+        main_y().wait_send()
+        for side in range(2):
+            for j in range(2):
+                edge_copy(side, j).wait_send()
+
+    @pl.when(helps)
+    def _():
+        for j in range(2):
+            far_copy(j).wait_send()
+    for side, at in ((0, 1), (1, n_sp - 2)):
+        @pl.when(sp == at)
+        def _(side=side):
+            rim_copy(side).wait_send()
+    for step in range(n_tp - 1):
+        stat_copy(step).wait_send()
+    df_copy(0, 0).wait_send()
+    for a, q in direct:
+        dg_copy(a, q).wait_send()
+        df_copy(a, q).wait_send()
+    for q in range(chips):
+        if q:
+            cg_copy(q).wait_send()
+        cf_copy(q).wait_send()
+
+
 def solution(mesh):
     n_grp, n_sp, n_tp = mesh.shape["grp"], mesh.shape["sp"], mesh.shape["tp"]
 
@@ -496,6 +1156,53 @@
         dma, vmem = pltpu.SemaphoreType.DMA, pltpu.VMEM
         anywhere = pl.BlockSpec(memory_space=pltpu.HBM)
         inside = pl.BlockSpec(memory_space=pltpu.VMEM)
+        if n_grp == 2 and n_sp >= 4 and n_tp % 2 == 0 and heads % 2 == 0 and channels % 256 == 0:
+            cols, ch, chips, steps = head_cols // 2, channels // 2, n_tp // 2, n_tp - 1
+            pieces = 4
+            scratch = [
+                vmem((length, width), BF16), vmem((4 * length, width), BF16),
+                vmem((width, cols), BF16), vmem((width, cols), BF16), vmem((width, cols), BF16),
+                vmem((width, 2 * ch), BF16), vmem((n_sp, 4 * heads, rows), BF16),
+                vmem((n_tp, columns, head_cols), BF16), vmem((n_tp, columns, channels), BF16),
+                vmem((pairs, length), F32),
+                vmem((heads, length, head_width), F32), vmem((pairs, length, 2 * head_width), BF16),
+                vmem((pairs, length, head_width), F32), vmem((pairs, length, head_width), F32),
+                vmem((pairs, length, length), F32), vmem((pairs, length, length), F32),
+                vmem((pairs, length, length), F32),
+                vmem((heads, length, head_width), F32), vmem((pairs, length, head_width), BF16),
+                vmem((pairs, head_width, head_width), BF16), vmem((pairs, head_width, head_width), F32),
+                vmem((2, heads, head_width, head_width), BF16), vmem((2, heads, head_width, head_width), BF16),
+                vmem((length, ch), BF16), vmem((2, length, ch), BF16), vmem((2, length, ch), BF16),
+                vmem((2, 2, HALO, ch), BF16),
+                vmem((2, length + 2 * HALO, ch), F32), vmem((length, channels), F32),
+                vmem((8, length), F32), vmem((steps, 8, length), F32),
+                vmem((n_tp, 2, length, cols), BF16), vmem((length, cols), BF16),
+                vmem((n_tp, length, channels), BF16),
+                dma((9,)),
+                dma((6, 2, n_sp - 1)), dma((6, 2, n_sp - 1)),
+                dma((2, pieces)), dma((2, pieces)), dma((3, pieces)), dma((3, pieces)),
+                dma((pieces,)), dma((pieces,)),
+                dma((1,)), dma((1,)), dma((2, steps)), dma((2, steps)), dma((2,)), dma((2,)),
+                dma((1,)), dma((2,)), dma((2, 2)), dma((2, 2)), dma((2,)), dma((2,)),
+                dma((steps,)), dma((steps,)),
+                dma((2, chips)), dma((2, chips)), dma((2, chips)), dma((2, chips)),
+                dma((chips,)), dma((chips,)), dma((chips,)), dma((chips,)),
+            ]
+            return pl.pallas_call(
+                functools.partial(fused, (n_sp, n_tp, float(channels * n_tp))),
+                out_shape=jax.ShapeDtypeStruct((length, columns), BF16),
+                in_specs=[anywhere, inside] + [anywhere] * 6 + [inside] * 5 + [anywhere] * 2,
+                out_specs=inside,
+                scratch_shapes=scratch,
+                compiler_params=pltpu.CompilerParams(
+                    collective_id=0, has_side_effects=True, vmem_limit_bytes=48 * 1024 * 1024
+                ),
+            )(
+                tokens_in, input_gain.reshape(1, width), w_key, w_gates.T, w_value, w_query,
+                w_glu_value, sigmoid_opener_matrix, log_decay.T,
+                head_gain.reshape(1, head_width), conv_kernel, norm_gain.reshape(1, channels),
+                norm_shift.reshape(1, channels), out_delta, out_conv,
+            )
         scratch = [
             vmem((length, width), BF16), vmem((length, width), BF16),
             vmem((width, head_cols), BF16), vmem((n_sp, 4 * heads, rows), BF16),

time: 84.4 us -> 77.7 us (0.921); the launches traced: 82.9 us -> 77.1 us
  Pallas kernels: 79.7 us -> 65.1 us
  local copies, waits for them, and re-layouts: 3.16 us -> 12 us
    pallas_call x1, Pallas kernels: 79.7 us -> 65.1 us  [on_device(): pl.pallas_call(functools.partial(fused, (n_sp, n_tp, float(channels * n_t...]
    unnamed x4 -> x31, local copies, waits for them, and re-layouts: 3.16 us -> 12 us
where the time goes in v1:
time: 77.7 us; the launch traced here: 77.1 us
  Pallas kernels  65.1 us (84%)
  local copies, waits for them, and re-layouts  12 us (15%)
    pallas_call x1, Pallas kernels, on_device(): pl.pallas_call(functools.partial(fused, (n_sp, n_tp, float(channels * n_t...  65.1 us
    unnamed x31, local copies, waits for them, and re-layouts  12 us

profile of v1, /device:TPU:0, one launch (start us, length us, event | category | flops | bytes accessed | tf_op | source)
XLA Modules:
  0.0 77.1 jit_solution(6668165552406408514)
XLA Ops:
  0.0 0.0 copy-start.9
  0.0 0.0 copy-start.13
  0.0 0.0 copy-start.12
  0.0 0.0 copy-start.14
  0.0 0.7 copy-done.9
  0.7 0.0 copy-done.13
  0.7 0.0 copy-done.12
  0.7 0.0 copy-done.14
  0.7 0.0 copy-start
  0.7 1.2 %copy-done = bf16[256,2048]{1,0:T(8,128)(2,1)S(1)} copy-done((bf16[256,2048]{1,0:T(8,128)(2,1)S(1)}, bf16[256,2048]{1,0:T(8,128)(2,1)}, u32[]{:S(2)}) %copy-start) | copy-done | bytes 1048600
  1.9 0.0 copy-start.1
  1.9 1.2 %copy-done.1 = bf16[2048,256]{1,0:T(8,128)(2,1)S(1)} copy-done((bf16[2048,256]{1,0:T(8,128)(2,1)S(1)}, bf16[2048,256]{1,0:T(8,128)(2,1)}, u32[]{:S(2)}) %copy-start.1) | copy-done | bytes 1048600
  3.2 0.0 copy-start.2
  3.2 1.2 %copy-done.2 = bf16[2048,256]{1,0:T(8,128)(2,1)S(1)} copy-done((bf16[2048,256]{1,0:T(8,128)(2,1)S(1)}, bf16[2048,256]{1,0:T(8,128)(2,1)}, u32[]{:S(2)}) %copy-start.2) | copy-done | bytes 1048600
  4.4 0.0 copy-start.3
  4.4 0.9 %copy-done.3 = bf16[512,256]{1,0:T(8,128)(2,1)S(1)} copy-done((bf16[512,256]{1,0:T(8,128)(2,1)S(1)}, bf16[512,256]{1,0:T(8,128)(2,1)}, u32[]{:S(2)}) %copy-start.3) | copy-done | bytes 262168
  5.3 0.0 copy-start.4
  5.3 0.9 %copy-done.4 = bf16[512,256]{1,0:T(8,128)(2,1)S(1)} copy-done((bf16[512,256]{1,0:T(8,128)(2,1)S(1)}, bf16[512,256]{1,0:T(8,128)(2,1)}, u32[]{:S(2)}) %copy-start.4) | copy-done | bytes 262168
  6.3 0.0 copy-start.5
  6.3 0.9 %copy-done.5 = bf16[512,256]{1,0:T(8,128)(2,1)S(1)} copy-done((bf16[512,256]{1,0:T(8,128)(2,1)S(1)}, bf16[512,256]{1,0:T(8,128)(2,1)}, u32[]{:S(2)}) %copy-start.5) | copy-done | bytes 262168
  7.2 0.0 copy-start.6
  7.2 0.9 %copy-done.6 = bf16[512,256]{1,0:T(8,128)(2,1)S(1)} copy-done((bf16[512,256]{1,0:T(8,128)(2,1)S(1)}, bf16[512,256]{1,0:T(8,128)(2,1)}, u32[]{:S(2)}) %copy-start.6) | copy-done | bytes 262168
  8.2 0.0 copy-start.7
  8.2 0.9 %copy-done.7 = bf16[512,256]{1,0:T(8,128)(2,1)S(1)} copy-done((bf16[512,256]{1,0:T(8,128)(2,1)S(1)}, bf16[512,256]{1,0:T(8,128)(2,1)}, u32[]{:S(2)}) %copy-start.7) | copy-done | bytes 262168
  9.1 0.0 copy-start.8
  9.1 0.8 copy-done.8
  9.9 0.0 copy-start.10
  9.9 0.7 copy-done.10
  10.6 0.0 copy-start.11
  10.6 0.7 copy-done.11
  11.3 65.1 %shard_map.145 = bf16[256,512]{1,0:T(8,128)(2,1)S(1)} custom-call(bf16[256,2048]{1,0:T(8,128)(2,1)S(1)} %copy-done, f32[1,2048]{1,0:T(1,128)S(1)} %bitcast.6, bf16[512,256]{1,0:T(8,128)(2,1)S(1)} %copy-done.3, bf16[8,512]{1,0:T(8,128)(2,1)S(1)} %bitcast.7, bf16[512,256]{1,0:T(8,128)(2,1)S(1)} %copy-done.4, bf16[512,256]{1,0:T(8,128)(2,1)S(1)} %copy-done.5, ...), custom_call_target="tpu_custom_call" | custom-call | tf_op jit(solution)/shard_map/pallas_call | solution.py:1191
  76.4 0.7 copy.17
Async XLA Ops:
  0.0 0.7 copy-start.9
  0.0 0.7 copy-start.13
  0.0 0.7 copy-start.12
  0.0 0.7 copy-start.14
  0.7 1.2 %copy-start = (bf16[256,2048]{1,0:T(8,128)(2,1)S(1)}, bf16[256,2048]{1,0:T(8,128)(2,1)}, u32[]{:S(2)}) copy-start(bf16[256,2048]{1,0:T(8,128)(2,1)} %tok_h.1) | copy-start | bytes 3145732
  1.9 1.2 %copy-start.1 = (bf16[2048,256]{1,0:T(8,128)(2,1)S(1)}, bf16[2048,256]{1,0:T(8,128)(2,1)}, u32[]{:S(2)}) copy-start(bf16[2048,256]{1,0:T(8,128)(2,1)} %od_h.1) | copy-start | bytes 3145732
  3.2 1.2 %copy-start.2 = (bf16[2048,256]{1,0:T(8,128)(2,1)S(1)}, bf16[2048,256]{1,0:T(8,128)(2,1)}, u32[]{:S(2)}) copy-start(bf16[2048,256]{1,0:T(8,128)(2,1)} %oc_h.1) | copy-start | bytes 3145732
  4.4 0.9 %copy-start.3 = (bf16[512,256]{1,0:T(8,128)(2,1)S(1)}, bf16[512,256]{1,0:T(8,128)(2,1)}, u32[]{:S(2)}) copy-start(bf16[512,256]{1,0:T(8,128)(2,1)} %wk_h.1) | copy-start | bytes 786436
  5.3 0.9 %copy-start.4 = (bf16[512,256]{1,0:T(8,128)(2,1)S(1)}, bf16[512,256]{1,0:T(8,128)(2,1)}, u32[]{:S(2)}) copy-start(bf16[512,256]{1,0:T(8,128)(2,1)} %wv_h.1) | copy-start | bytes 786436
  6.3 0.9 %copy-start.5 = (bf16[512,256]{1,0:T(8,128)(2,1)S(1)}, bf16[512,256]{1,0:T(8,128)(2,1)}, u32[]{:S(2)}) copy-start(bf16[512,256]{1,0:T(8,128)(2,1)} %wq_h.1) | copy-start | bytes 786436
  7.2 0.9 %copy-start.6 = (bf16[512,256]{1,0:T(8,128)(2,1)S(1)}, bf16[512,256]{1,0:T(8,128)(2,1)}, u32[]{:S(2)}) copy-start(bf16[512,256]{1,0:T(8,128)(2,1)} %wa_h.1) | copy-start | bytes 786436
  8.2 0.9 %copy-start.7 = (bf16[512,256]{1,0:T(8,128)(2,1)S(1)}, bf16[512,256]{1,0:T(8,128)(2,1)}, u32[]{:S(2)}) copy-start(bf16[512,256]{1,0:T(8,128)(2,1)} %wb_h.1) | copy-start | bytes 786436
  9.1 0.8 copy-start.8
  9.9 0.7 copy-start.10
  10.6 0.7 copy-start.11

commit v2 on v1

--- a/solution.py
+++ b/solution.py
@@ -484,7 +484,7 @@
           tok, nt, wk, wv, wq, wab, wg, odg, ocg, ldo,
           keys, vals, betas, cums, xinv, gaps, rhs, local_out, reads, maps, ends,
           chain_in, chain_out, gout, gend, main_in, edge_in, pad, conv, stat_out, stat_in,
-          dall, dm_out, call,
+          dall, dm_out, call, acc_ab, acc_q,
           local_sem, z_send, z_recv, ty_send, ty_recv, tf_send, tf_recv, tz_send, tz_recv,
           ld_send, ld_recv, od_send, od_recv, chain_send, chain_recv,
           main_send, main_recv, edge_send, edge_recv, far_send, rim_send,
@@ -518,16 +518,23 @@
             src_ref=src, dst_ref=dst, send_sem=send, recv_sem=recv, device_id=where, device_id_type=MESH
         )
 
-    def source(w):
+    halves = z_send.shape[3]
+    slab = rows // halves
+
+    def source(w, k=None):
         if w == GATE:
             return wg_h
         size = channels if w in (GLU, OPEN) else cols
-        return sources[w].at[:, pl.ds(pl.multiple_of(grp * size, 128), size)]
-
-    def target(w, index):
+        lanes = pl.ds(pl.multiple_of(grp * size, 128), size)
+        return sources[w].at[:, lanes] if k is None else sources[w].at[pl.ds(k * slab, slab), lanes]
+
+    def target(w, index, k=None):
         if w == GATE:
             return wg.at[index]
-        at = pl.ds(pl.multiple_of(index * rows, 16), rows)
+        if k is None:
+            at = pl.ds(pl.multiple_of(index * rows, 16), rows)
+        else:
+            at = pl.ds(pl.multiple_of(index * rows + k * slab, 16), slab)
         if w in (GLU, OPEN):
             return wab.at[at, pl.ds(channels if w == OPEN else 0, channels)]
         return plain[w].at[at]
@@ -599,18 +606,22 @@
             return (sp - (d - 1) >= 0) & (sp < n_sp - 1 - wide(w))
         return (sp + (d - 1) < n_sp) & (sp > wide(w))
 
-    def z_copy(w, side, d):
+    def cuts(w):
+        return range(1 if w == GATE else halves)
+
+    def z_copy(w, side, d, k):
         back = d - 1
-        place = target(w, sp - back if side == 0 else sp + back)
+        place = target(w, sp - back if side == 0 else sp + back, k)
         return remote(
-            source(w) if d == 1 else place, place, z_send.at[w, side, d - 1], z_recv.at[w, side, d - 1],
+            source(w, k) if d == 1 else place, place,
+            z_send.at[w, side, d - 1, k], z_recv.at[w, side, d - 1, k],
             sp=sp + 1 if side == 0 else sp - 1,
         )
 
-    def z_arrival(w, side, d):
-        place = target(w, sp - d if side == 0 else sp + d)
+    def z_arrival(w, side, d, k):
+        place = target(w, sp - d if side == 0 else sp + d, k)
         return remote(
-            place, place, z_send.at[w, side, d - 1], z_recv.at[w, side, d - 1],
+            place, place, z_send.at[w, side, d - 1, k], z_recv.at[w, side, d - 1, k],
             sp=sp + 1 if side == 0 else sp - 1,
         )
 
@@ -618,19 +629,21 @@
         for side in range(2):
             @pl.when(leaves(w, side, 1) & where)
             def _(side=side):
-                z_copy(w, side, 1).start()
+                for k in cuts(w):
+                    z_copy(w, side, 1, k).start()
 
     def relay(w, d):
         if d > n_sp - 1:
             return
-        for side in range(2):
-            @pl.when(arrives(w, side, d))
-            def _(side=side):
-                z_arrival(w, side, d).wait_recv()
-                if d < n_sp - 1:
-                    @pl.when(leaves(w, side, d + 1))
-                    def _():
-                        z_copy(w, side, d + 1).start()
+        for k in cuts(w):
+            for side in range(2):
+                @pl.when(arrives(w, side, d))
+                def _(side=side, k=k):
+                    z_arrival(w, side, d, k).wait_recv()
+                    if d < n_sp - 1:
+                        @pl.when(leaves(w, side, d + 1))
+                        def _():
+                            z_copy(w, side, d + 1, k).start()
 
     pieces = ty_send.shape[1]
     half = length // 2
@@ -713,18 +726,20 @@
 
     relay(GATE, 1)
     relay(KEY, 1)
+    offer(GLU, inner)
+    pass_y(0, 0)
     relay(GATE, 2)
+    relay(VALUE, 1)
+    pass_y(0, 1)
+    offer(OPEN, inner)
     relay(KEY, 2)
-    relay(VALUE, 1)
-    offer(GLU, inner)
+    pass_y(0, 2)
+    relay(GLU, 1)
+    offer(QUERY, inner)
+    pass_y(0, 3)
     for d in range(3, n_sp):
         relay(GATE, d)
         relay(KEY, d)
-    relay(GLU, 1)
-    offer(OPEN, inner)
-    offer(QUERY, inner)
-    for c in range(pieces):
-        pass_y(0, c)
     pass_z(0)
     own[GATE].wait()
     own[KEY].wait()
@@ -778,10 +793,9 @@
 
     service = {
         2: [lambda: pass_z(2), lambda: pass_far(0)],
-        8: [lambda: pass_z(3), lambda: pass_far(1)],
-        32: [lambda: pass_far(2)],
-        64: [lambda: relay(GLU, 2)],
-        128: [lambda: pass_far(3), lambda: relay(OPEN, 1)],
+        8: [lambda: pass_far(1)],
+        32: [lambda: pass_z(3)],
+        128: [lambda: pass_far(2)],
     }
     size = 2
     while size < length:
@@ -843,15 +857,55 @@
                     chain_copy(r).start()
 
     chain_point(0, 0)
-    for d in range(3, n_sp):
+    relay(OPEN, 1)
+    pass_far(3)
+    relay(QUERY, 1)
+    chain_point(1, 1)
+
+    def block_dot(first, count, w_ref, index):
+        lanes = pl.ds(pl.multiple_of(index * rows, 128), rows)
+        at = pl.ds(pl.multiple_of(index * rows, 128), rows)
+        return dot(nt[first * length:(first + count) * length, lanes], w_ref[at, :])
+
+    def neighbours(w, d, action):
+        for side in range(2):
+            @pl.when(arrives(w, side, d))
+            def _(side=side):
+                action(sp - d if side == 0 else sp + d)
+
+    def add_wide(index, fresh=False):
+        x = block_dot(0, 2, wab, index)
+        acc_ab[0:both, :] = x if fresh else acc_ab[0:both, :] + x
+
+        @pl.when(helps)
+        def _():
+            y = block_dot(2, 2, wab, index)
+            acc_ab[both:, :] = y if fresh else acc_ab[both:, :] + y
+
+    def add_query(index, fresh=False):
+        x = block_dot(0, 2, wq, index)
+        acc_q[...] = x if fresh else acc_q[...] + x
+
+    @pl.when(inner)
+    def _():
+        own[GLU].wait()
+        own[OPEN].wait()
+
+        @pl.when(helps)
+        def _():
+            for c in range(pieces):
+                tok_f_arrival(2, c).wait_recv()
+                tok_f_arrival(3, c).wait_recv()
+
+        add_wide(sp, True)
+    neighbours(GLU, 1, add_wide)
+    for d in range(2, n_sp - 1):
         relay(GLU, d)
-    relay(QUERY, 1)
-    relay(OPEN, 2)
-    for d in range(3, n_sp):
         relay(OPEN, d)
+        neighbours(GLU, d, add_wide)
 
     def gated(first, count):
-        x = dot(nt[first * length:(first + count) * length, :], wab[...])
+        x = acc_ab[first * length:(first + count) * length, :]
         return (x[:, :channels] * jax.nn.sigmoid(x[:, channels:])).astype(BF16)
 
     def owner(j):
@@ -886,14 +940,8 @@
 
     @pl.when(inner)
     def _():
-        own[GLU].wait()
-        own[OPEN].wait()
-
         @pl.when(helps)
         def _():
-            for c in range(pieces):
-                tok_f_arrival(2, c).wait_recv()
-                tok_f_arrival(3, c).wait_recv()
             far = gated(2, 2)
             gend[0] = far[:length]
             gend[1] = far[length:]
@@ -914,11 +962,13 @@
             for j in range(2):
                 edge_copy(side, j).start()
 
-    chain_point(1, 1)
-    relay(QUERY, 2)
-    for at in range(2, n_sp - 1):
-        chain_point(at, at)
-        relay(QUERY, at + 1)
+    own[QUERY].wait()
+    add_query(sp, True)
+    neighbours(QUERY, 1, add_query)
+    for d in range(2, n_sp - 1):
+        chain_point(d, d)
+        relay(QUERY, d)
+        neighbours(QUERY, d, add_query)
     chain_point(n_sp - 1, n_sp - 1)
 
     for h in range(2):
@@ -968,10 +1018,12 @@
     for step in range(n_tp - 1):
         stat_copy(step).start()
 
-    own[QUERY].wait()
-    query_proj = silu(dot(nt[0:both, :], wq[...]))
-    for u, (j, h) in enumerate(units):
-        query = query_proj[j * length:(j + 1) * length, h * head_width:(h + 1) * head_width]
+    relay(QUERY, n_sp - 1)
+    neighbours(QUERY, n_sp - 1, add_query)
+
+    def read(u):
+        j, h = units[u]
+        query = silu(acc_q[j * length:(j + 1) * length, h * head_width:(h + 1) * head_width])
         query = unit_rows(query) * head_width ** -0.5
         scores = bdot(query, keys[u], NT)
         for r in range(2):
@@ -1026,10 +1078,12 @@
     direct = [(a, q) for q in range(chips) for a in (1, 0) if (a, q) != (0, 0)]
 
     for h in range(heads):
+        read(heads + h)
         dm_out[:, h * head_width:(h + 1) * head_width] = mixed_head(heads + h)
     for q in range(chips - 1, -1, -1):
         dg_copy(1, q).start()
     for h in range(heads):
+        read(h)
         dall[tp, grp, :, h * head_width:(h + 1) * head_width] = mixed_head(h)
     for q in range(1, chips):
         dg_copy(0, q).start()
@@ -1089,7 +1143,8 @@
             for side in range(2):
                 @pl.when(leaves(w, side, d))
                 def _(w=w, d=d, side=side):
-                    z_copy(w, side, d).wait_send()
+                    for k in cuts(w):
+                        z_copy(w, side, d, k).wait_send()
     for c in range(pieces):
         tok_y(0, c).wait_send()
         tok_f(1, c).wait_send()
@@ -1177,9 +1232,9 @@
                 vmem((2, length + 2 * HALO, ch), F32), vmem((length, channels), F32),
                 vmem((8, length), F32), vmem((steps, 8, length), F32),
                 vmem((n_tp, 2, length, cols), BF16), vmem((length, cols), BF16),
-                vmem((n_tp, length, channels), BF16),
+                vmem((n_tp, length, channels), BF16), vmem((4 * length, 2 * ch), F32), vmem((2 * length, cols), F32),
                 dma((9,)),
-                dma((6, 2, n_sp - 1)), dma((6, 2, n_sp - 1)),
+                dma((6, 2, n_sp - 1, 2)), dma((6, 2, n_sp - 1, 2)),
                 dma((2, pieces)), dma((2, pieces)), dma((3, pieces)), dma((3, pieces)),
                 dma((pieces,)), dma((pieces,)),
                 dma((1,)), dma((1,)), dma((2, steps)), dma((2, steps)), dma((2,)), dma((2,)),
@@ -1195,7 +1250,7 @@
                 out_specs=inside,
                 scratch_shapes=scratch,
                 compiler_params=pltpu.CompilerParams(
-                    collective_id=0, has_side_effects=True, vmem_limit_bytes=48 * 1024 * 1024
+                    collective_id=0, has_side_effects=True, vmem_limit_bytes=58 * 1024 * 1024
                 ),
             )(
                 tokens_in, input_gain.reshape(1, width), w_key, w_gates.T, w_value, w_query,

time: 77.7 us -> 60.4 us (0.78)
  local copies, waits for them, and re-layouts: 12 us -> 1.67 us
  Pallas kernels: 65.1 us -> 58.5 us
    unnamed x31 -> x1, local copies, waits for them, and re-layouts: 12 us -> 1.67 us
    pallas_call x1, Pallas kernels: 65.1 us -> 58.5 us  [on_device(): pl.pallas_call(functools.partial(fused, (n_sp, n_tp, float(channels * n_t...]
where the time goes in v2:
time: 60.4 us; the launch traced here: 60.1 us
  Pallas kernels  58.5 us (97%)
  local copies, waits for them, and re-layouts  1.67 us (3%)
    pallas_call x1, Pallas kernels, on_device(): pl.pallas_call(functools.partial(fused, (n_sp, n_tp, float(channels * n_t...  58.5 us
    unnamed x1, local copies, waits for them, and re-layouts  1.67 us

profile of v2, /device:TPU:0, one launch (start us, length us, event | category | flops | bytes accessed | tf_op | source)
XLA Modules:
  0.0 60.1 jit_solution(8635579240159698448)
XLA Ops:
  0.0 58.5 %shard_map.145 = bf16[256,512]{1,0:T(8,128)(2,1)} custom-call(bf16[256,2048]{1,0:T(8,128)(2,1)} %tok_h.1, f32[1,2048]{1,0:T(1,128)} %bitcast.6, bf16[512,256]{1,0:T(8,128)(2,1)} %wk_h.1, bf16[8,512]{1,0:T(8,128)(2,1)} %bitcast.7, bf16[512,256]{1,0:T(8,128)(2,1)} %wv_h.1, bf16[512,256]{1,0:T(8,128)(2,1)} %wq_h.1, bf16[512,256]{1,0:T(8,128)(2,1)} %wa_h.1, ...), custom_call_target="tpu_custom_call" | custom-call | tf_op jit(solution)/shard_map/pallas_call | solution.py:1246
  58.5 1.7 %copy.17 = bf16[256,512]{1,0:T(8,128)(2,1)} copy(bf16[256,512]{1,0:T(8,128)(2,1)} %shard_map.145) | data formatting | bytes 524288

commit v3 on v1

--- a/solution.py
+++ b/solution.py
@@ -479,13 +479,14 @@
             part_copy(p).wait_send()
 
 
-def fused(cfg, tok_h, gain, wk_h, wg_h, wv_h, wq_h, wa_h, wb_h, ldt, hgain, ck, ng, ns, od_h, oc_h,
+def fused(cfg, tok_h, gain_h, wk_h, wg_h, wv_h, wq_h, wa_h, wb_h, ldt_h, hgain_h, ck_h, ng_h, ns_h, od_h, oc_h,
           out,
+          gain, ldt, hgain, ck, ng, ns,
           tok, nt, wk, wv, wq, wab, wg, odg, ocg, ldo,
           keys, vals, betas, cums, xinv, gaps, rhs, local_out, reads, maps, ends,
           chain_in, chain_out, gout, gend, main_in, edge_in, pad, conv, stat_out, stat_in,
-          dall, dm_out, call,
-          local_sem, z_send, z_recv, ty_send, ty_recv, tf_send, tf_recv, tz_send, tz_recv,
+          dall, dm_out, call, acc_ab, acc_q, acc_k, acc_v,
+          local_sem, g_send, g_recv, z_send, z_recv, ty_send, ty_recv, tx_recv, tf_send, tf_recv, tz_send, tz_recv,
           ld_send, ld_recv, od_send, od_recv, chain_send, chain_recv,
           main_send, main_recv, edge_send, edge_recv, far_send, rim_send,
           stat_send, stat_recv, dg_send, dg_recv, df_send, df_recv, cg_send, cg_recv, cf_send, cf_recv):
@@ -518,38 +519,26 @@
             src_ref=src, dst_ref=dst, send_sem=send, recv_sem=recv, device_id=where, device_id_type=MESH
         )
 
+    counts = (4, 1, 2, 2, 2, 2)
+    firsts = (0, 0, 4, 6, 8, 10)
+
     def source(w):
         if w == GATE:
             return wg_h
         size = channels if w in (GLU, OPEN) else cols
         return sources[w].at[:, pl.ds(pl.multiple_of(grp * size, 128), size)]
 
-    def target(w, index):
+    def target(w, index, k=None):
         if w == GATE:
             return wg.at[index]
-        at = pl.ds(pl.multiple_of(index * rows, 16), rows)
+        slab = rows // counts[w]
+        if k is None:
+            at = pl.ds(pl.multiple_of(index * rows, 16), rows)
+        else:
+            at = pl.ds(pl.multiple_of(index * rows + k * slab, 16), slab)
         if w in (GLU, OPEN):
             return wab.at[at, pl.ds(channels if w == OPEN else 0, channels)]
         return plain[w].at[at]
-
-    load_tok = pltpu.make_async_copy(tok_h, tok, local_sem.at[0])
-    load_tok.start()
-    own = [pltpu.make_async_copy(source(w), target(w, sp), local_sem.at[1 + w]) for w in range(6)]
-    for w in (KEY, GATE, VALUE, QUERY):
-        own[w].start()
-
-    @pl.when(inner)
-    def _():
-        own[GLU].start()
-        own[OPEN].start()
-
-    def od_rows(index):
-        return pl.ds(pl.multiple_of(index * columns, 16), columns)
-
-    load_od = pltpu.make_async_copy(od_h.at[od_rows(tp)], odg.at[tp], local_sem.at[7])
-    load_oc = pltpu.make_async_copy(oc_h.at[od_rows(tp)], ocg.at[tp], local_sem.at[8])
-    load_od.start()
-    load_oc.start()
 
     barrier = pltpu.get_barrier_semaphore()
 
@@ -572,13 +561,40 @@
         greet(sp=sp + 1)
         greet(sp=sp + 1, grp=other)
 
+    load_tok = pltpu.make_async_copy(tok_h, tok, local_sem.at[0])
+    load_tok.start()
+    small = [
+        pltpu.make_async_copy(src, dst, local_sem.at[9 + i])
+        for i, (src, dst) in enumerate(
+            ((gain_h, gain), (ldt_h, ldt), (hgain_h, hgain), (ck_h, ck), (ng_h, ng), (ns_h, ns))
+        )
+    ]
+    for copy in small:
+        copy.start()
+    own = [pltpu.make_async_copy(source(w), target(w, sp), local_sem.at[1 + w]) for w in range(6)]
+    for copy in own:
+        copy.start()
+
+    def od_rows(index):
+        return pl.ds(pl.multiple_of(index * columns, 16), columns)
+
+    load_od = pltpu.make_async_copy(od_h.at[od_rows(tp)], odg.at[tp], local_sem.at[7])
+    load_oc = pltpu.make_async_copy(oc_h.at[od_rows(tp)], ocg.at[tp], local_sem.at[8])
+    load_od.start()
+    load_oc.start()
+
     load_tok.wait()
+    for copy in small:
+        copy.wait()
     chunk = 64
     for at in range(0, length, chunk):
         here = tok[at:at + chunk, :].astype(F32)
         scale = lax.rsqrt(jnp.mean(here * here, axis=-1, keepdims=True) + EPSILON)
         nt[at:at + chunk, :] = (here * scale * gain[...]).astype(BF16)
 
+    for w in (GATE, KEY):
+        own[w].wait()
+
     @pl.when(edge)
     def _():
         pl.semaphore_wait(barrier, 2 * n_tp + 1)
@@ -599,60 +615,87 @@
             return (sp - (d - 1) >= 0) & (sp < n_sp - 1 - wide(w))
         return (sp + (d - 1) < n_sp) & (sp > wide(w))
 
-    def z_copy(w, side, d):
-        back = d - 1
-        place = target(w, sp - back if side == 0 else sp + back)
-        return remote(
-            source(w) if d == 1 else place, place, z_send.at[w, side, d - 1], z_recv.at[w, side, d - 1],
-            sp=sp + 1 if side == 0 else sp - 1,
-        )
-
-    def z_arrival(w, side, d):
-        place = target(w, sp - d if side == 0 else sp + d)
-        return remote(
-            place, place, z_send.at[w, side, d - 1], z_recv.at[w, side, d - 1],
-            sp=sp + 1 if side == 0 else sp - 1,
-        )
-
-    def offer(w, where):
+    def origin(side, d):
+        return sp - d if side == 0 else sp + d
+
+    def z_block(w, index, side, k):
+        place = target(w, index, k)
+        if w == GATE:
+            send, recv = g_send.at[side], g_recv.at[index]
+        else:
+            send, recv = z_send.at[side], z_recv.at[index, firsts[w] + k]
+        return remote(place, place, send, recv, sp=sp + 1 if side == 0 else sp - 1)
+
+    def cuts(w):
+        return range(counts[w])
+
+    def offer(w, where, ks=None):
         for side in range(2):
             @pl.when(leaves(w, side, 1) & where)
             def _(side=side):
-                z_copy(w, side, 1).start()
-
-    def relay(w, d):
+                for k in cuts(w) if ks is None else ks:
+                    z_block(w, sp, side, k).start()
+
+    def from_edge(side, d):
+        return (sp - d == 0) if side == 0 else (sp + d == n_sp - 1)
+
+    def relay(w, d, kind=None, ks=None):
         if d > n_sp - 1:
             return
-        for side in range(2):
-            @pl.when(arrives(w, side, d))
-            def _(side=side):
-                z_arrival(w, side, d).wait_recv()
-                if d < n_sp - 1:
-                    @pl.when(leaves(w, side, d + 1))
-                    def _():
-                        z_copy(w, side, d + 1).start()
-
-    pieces = ty_send.shape[1]
+        for k in cuts(w) if ks is None else ks:
+            for side in range(2):
+                onward = leaves(w, side, d + 1) if d < n_sp - 1 else sp < 0
+                here = arrives(w, side, d) & onward
+                if kind == "edge":
+                    here = here & from_edge(side, d)
+                if kind == "inner":
+                    here = here & ~from_edge(side, d)
+
+                @pl.when(here)
+                def _(side=side, k=k):
+                    z_block(w, origin(side, d), side, k).wait_recv()
+                    z_block(w, origin(side, d), side, k).start()
+
+    def drain(w, d):
+        for k in cuts(w):
+            for side in range(2):
+                onward = leaves(w, side, d + 1) if d < n_sp - 1 else sp < 0
+
+                @pl.when(arrives(w, side, d) & ~onward)
+                def _(side=side, k=k):
+                    z_block(w, origin(side, d), side, k).wait_recv()
+
+    pieces = ty_recv.shape[0]
     half = length // 2
     piece = half // pieces
+    grains = tz_recv.shape[0]
+    grain = half // grains
 
     def part(block, side, c):
-        return nt.at[pl.ds(pl.multiple_of(block * length + side * half + c * piece, 16), piece)]
+        size = grain if block > 1 else piece
+        return nt.at[pl.ds(pl.multiple_of(block * length + side * half + c * size, 16), size)]
 
     def tok_y(k, c):
-        return remote(part(2 * k, core, c), part(2 * k + 1, core, c), ty_send.at[k, c], ty_recv.at[k, c], grp=other)
+        return remote(
+            part(2 * k, core, c), part(2 * k + 1, core, c), ty_send.at[k], (ty_recv, tx_recv)[k].at[c], grp=other
+        )
 
     def tok_z(c):
-        return remote(part(0, core, c), part(2, core, c), tz_send.at[c], tz_recv.at[c], sp=helper)
+        src = nt.at[pl.ds(pl.multiple_of(core * half + c * grain, 16), grain)]
+        return remote(src, part(2, core, c), tz_send.at[0], tz_recv.at[c], sp=helper)
 
     def tok_f(block, c):
         return remote(
-            part(block, core, c), part(block, core, c), tf_send.at[block - 1, c], tf_recv.at[block - 1, c], tp=sibling
-        )
-
-    def tok_f_arrival(block, c):
-        place = part(block, 1 - core, c)
-        return remote(place, place, tf_send.at[block - 1, c], tf_recv.at[block - 1, c], tp=sibling)
+            part(block, core, c), part(block, core, c), tf_send.at[block - 1], tf_recv.at[block - 1], tp=sibling
+        )
+
+    def tok_f_arrival(block):
+        place = nt.at[pl.ds(pl.multiple_of(block * length + (1 - core) * half, 16), half)]
+        return remote(place, place, tf_send.at[block - 1], tf_recv.at[block - 1], tp=sibling)
+
+    def half_rows(send):
+        place = nt.at[pl.ds(0, half)]
+        return remote(place, place, send, send, tp=sibling)
 
     def pass_y(k, c):
         tok_y(k, c).wait_recv()
@@ -675,12 +718,11 @@
     def od_copy(m, step):
         dest = lax.rem(tp + step + 1, n_tp)
         src, dst = ((od_h, odg), (oc_h, ocg))[m]
-        return remote(src.at[od_rows(dest)], dst.at[tp], od_send.at[m, step], od_recv.at[m, step], tp=dest)
-
-    def od_arrival(m, step):
-        origin = lax.rem(tp + n_tp - step - 1, n_tp)
-        place = (odg, ocg)[m].at[origin]
-        return remote(place, place, od_send.at[m, step], od_recv.at[m, step], tp=origin)
+        return remote(src.at[od_rows(dest)], dst.at[tp], od_send.at[m], od_recv.at[m], tp=dest)
+
+    def od_all(m):
+        place = (odg, ocg)[m].at[pl.ds(0, n_tp - 1)]
+        return remote(place, place, od_send.at[m], od_recv.at[m], tp=sibling)
 
     everywhere = sp >= 0
     offer(GATE, everywhere)
@@ -688,15 +730,17 @@
     for c in range(pieces):
         tok_y(0, c).start()
     ld_copy.start()
-    offer(VALUE, everywhere)
+    for w in (VALUE, GLU, OPEN, QUERY):
+        own[w].wait()
+    offer(VALUE, edge)
     offer(GLU, edge)
+    offer(OPEN, edge)
 
     @pl.when(edge)
     def _():
-        for c in range(pieces):
+        for c in range(grains):
             tok_z(c).start()
 
-    offer(OPEN, edge)
     offer(QUERY, edge)
     for m in (1, 0):
         for step in range(n_tp - 1):
@@ -711,77 +755,128 @@
     def silu(tensor):
         return tensor * jax.nn.sigmoid(tensor)
 
-    relay(GATE, 1)
-    relay(KEY, 1)
-    relay(GATE, 2)
-    relay(KEY, 2)
-    relay(VALUE, 1)
-    offer(GLU, inner)
-    for d in range(3, n_sp):
-        relay(GATE, d)
-        relay(KEY, d)
-    relay(GLU, 1)
-    offer(OPEN, inner)
-    offer(QUERY, inner)
-    for c in range(pieces):
-        pass_y(0, c)
-    pass_z(0)
-    own[GATE].wait()
-    own[KEY].wait()
-    ld_copy.wait_recv()
-    for c in range(pieces):
-        tok_f_arrival(1, c).wait_recv()
-
-    both = 2 * length
-    gate_cols = jnp.zeros((both, wg.shape[1]), F32)
-    gate_rows = jnp.zeros((wg.shape[1], both), F32)
-    for index in range(n_sp):
-        normed_part = nt[0:both, index * rows:(index + 1) * rows]
-        gate_cols = gate_cols + dot(normed_part, wg[index], NT)
-        gate_rows = gate_rows + dot(wg[index], normed_part, NT)
-    mine = grp == 0
-    gates = 4 * heads
-    gate_cols = jnp.where(mine, gate_cols[:, :gates], gate_cols[:, gates:])
-    gate_rows = jnp.where(mine, gate_rows[:gates, :], gate_rows[gates:, :])
-    rates = [
-        jnp.where(mine, log[:2 * heads, :], log[2 * heads:, :]) for log in (ldt[...], ldo[...])
-    ]
+    def block_dot(first, count, w_ref, index):
+        lanes = pl.ds(pl.multiple_of(index * rows, 128), rows)
+        at = pl.ds(pl.multiple_of(index * rows, 128), rows)
+        return dot(nt[first * length:(first + count) * length, lanes], w_ref[at, :])
+
+    def neighbours(w, d, action):
+        for side in range(2):
+            @pl.when(arrives(w, side, d))
+            def _(side=side):
+                action(sp - d if side == 0 else sp + d)
+
+    def adder(acc, w_ref, first, count):
+        span = slice(first * length, (first + count) * length)
+
+        def add(index, fresh=False):
+            x = block_dot(first, count, w_ref, index)
+            acc[span, :] = x if fresh else acc[span, :] + x
+
+        return add
 
     row_at = lax.broadcasted_iota(jnp.int32, (length, length), 0)
     col_at = lax.broadcasted_iota(jnp.int32, (length, length), 1)
     same = row_at == col_at
-
-    key_proj = silu(dot(nt[0:both, :], wk[...]))
+    mine = grp == 0
+    gates = 4 * heads
+
+    def weights_of(j):
+        span = slice(j * length, (j + 1) * length)
+        cols_part = jnp.zeros((length, wg.shape[1]), F32)
+        for index in range(n_sp):
+            cols_part = cols_part + dot(nt[span, index * rows:(index + 1) * rows], wg[index], NT)
+        rows_part = jnp.transpose(cols_part)
+        gate_cols = jnp.where(mine, cols_part[:, :gates], cols_part[:, gates:])
+        gate_rows = jnp.where(mine, rows_part[:gates, :], rows_part[gates:, :])
+        log = (ldt, ldo)[j]
+        rates = jnp.where(mine, log[:2 * heads, :], log[2 * heads:, :])
+        for h in range(heads):
+            for r in range(2):
+                p = 2 * (j * heads + h) + r
+                g = 4 * h + 2 * r
+                decay_row = rates[2 * h + r:2 * h + r + 1, :] * (0.5 + jax.nn.sigmoid(gate_rows[g:g + 1, :]))
+                beta = jax.nn.sigmoid(gate_cols[:, g + 1:g + 2] - BETA_SHIFT)
+                seen = col_at <= row_at if r == 0 else col_at >= row_at
+                cum_col = jnp.sum(jnp.where(seen, decay_row, 0.0), axis=1, keepdims=True)
+                cum_row = jnp.sum(jnp.where(same, cum_col, 0.0), axis=0, keepdims=True)
+                gaps[p] = jnp.where(seen, jnp.exp(jnp.where(seen, cum_col - cum_row, 0.0)), 0.0)
+                betas[p] = jnp.broadcast_to(beta, (length, head_width))
+                cums[p] = jnp.broadcast_to(cum_col, (length, head_width))
+
+    add_key = [adder(acc_k, wk, j, 1) for j in range(2)]
+    add_value = [adder(acc_v, wv, j, 1) for j in range(2)]
+
+    relay(GATE, 1)
+    relay(KEY, 1, None, (0, 1))
+    offer(VALUE, inner, (0,))
+    relay(KEY, 1, None, (2, 3))
+    offer(VALUE, inner, (1,))
+    relay(GATE, 2)
+    pass_y(0, 0)
+    for d in range(2, n_sp - 1):
+        relay(KEY, d, None, (0, 1))
+    relay(VALUE, 1, None, (0,))
+    for d in range(2, n_sp - 1):
+        relay(KEY, d, None, (2, 3))
+    offer(GLU, inner)
+    pass_y(0, 1)
+    relay(VALUE, 1, None, (1,))
+    offer(OPEN, inner)
+    def pass_value():
+        for d in range(2, n_sp - 1):
+            relay(VALUE, d)
+
+    drain(KEY, 1)
+    add_key[0](sp, True)
+    neighbours(KEY, 1, add_key[0])
+    pass_y(0, 2)
+    offer(QUERY, inner)
+    drain(VALUE, 1)
+    add_value[0](sp, True)
+    neighbours(VALUE, 1, add_value[0])
+    relay(GLU, 1)
+    for d in range(1, n_sp):
+        drain(GATE, d)
+    weights_of(0)
+    pass_y(0, 3)
+    for d in range(2, n_sp - 1):
+        drain(KEY, d)
+        neighbours(KEY, d, add_key[0])
+    ld_copy.wait_recv()
+    tok_f_arrival(1).wait_recv()
+    relay(OPEN, 1)
+    weights_of(1)
+    pass_z(0)
+    pass_value()
+    add_key[1](sp, True)
+    for d in range(1, n_sp - 1):
+        neighbours(KEY, d, add_key[1])
+    add_value[1](sp, True)
+    neighbours(VALUE, 1, add_value[1])
     pass_z(1)
-    relay(VALUE, 2)
+    drain(KEY, n_sp - 1)
+    neighbours(KEY, n_sp - 1, adder(acc_k, wk, 0, 2))
+
+    both = 2 * length
+    key_proj = silu(acc_k[...])
     for u, (j, h) in enumerate(units):
         keys[u] = unit_rows(key_proj[j * length:(j + 1) * length, h * head_width:(h + 1) * head_width])
-    for u, (j, h) in enumerate(units):
+    near = row_at // 2 == col_at // 2
+    for u in range(n_units):
         grams = bdot(keys[u], keys[u], NT)
         for r in range(2):
             p = 2 * u + r
-            g = 4 * h + 2 * r
-            span = slice(j * length, (j + 1) * length)
-            decay_row = rates[j][2 * h + r:2 * h + r + 1, :] * (0.5 + jax.nn.sigmoid(gate_rows[g:g + 1, span]))
-            beta = jax.nn.sigmoid(gate_cols[span, g + 1:g + 2] - BETA_SHIFT)
-            seen = col_at <= row_at if r == 0 else col_at >= row_at
-            cum_col = jnp.sum(jnp.where(seen, decay_row, 0.0), axis=1, keepdims=True)
-            cum_row = jnp.sum(jnp.where(same, cum_col, 0.0), axis=0, keepdims=True)
-            weighting = jnp.where(seen, jnp.exp(jnp.where(seen, cum_col - cum_row, 0.0)), 0.0)
-            gaps[p] = weighting
-            betas[p] = jnp.broadcast_to(beta, (length, head_width))
-            cums[p] = jnp.broadcast_to(cum_col, (length, head_width))
-            lower = jnp.where(same, 0.0, grams * weighting * beta)
+            beta = jnp.concatenate([betas[p]] * (length // head_width), axis=1)
+            lower = jnp.where(same, 0.0, grams * gaps[p] * beta)
             rhs[p] = lower
-            near = (row_at // 2 == col_at // 2)
             xinv[p] = jnp.where(same, 1.0, jnp.where(near, -lower, 0.0))
 
     service = {
-        2: [lambda: pass_z(2), lambda: pass_far(0)],
-        8: [lambda: pass_z(3), lambda: pass_far(1)],
-        32: [lambda: pass_far(2)],
-        64: [lambda: relay(GLU, 2)],
-        128: [lambda: pass_far(3), lambda: relay(OPEN, 1)],
+        4: [lambda: pass_z(2)],
+        8: [lambda: pass_z(3)],
+        32: [lambda: pass_z(4)],
+        128: [lambda: pass_z(5)],
     }
     size = 2
     while size < length:
@@ -794,10 +889,10 @@
             act()
         size *= 2
 
-    own[VALUE].wait()
-    for d in range(3, n_sp):
-        relay(VALUE, d)
-    value_proj = silu(dot(nt[0:both, :], wv[...]))
+    for d in range(2, n_sp):
+        drain(VALUE, d)
+        neighbours(VALUE, d, adder(acc_v, wv, 0, 2))
+    value_proj = silu(acc_v[...])
     eye = (
         lax.broadcasted_iota(jnp.int32, (head_width, head_width), 0)
         == lax.broadcasted_iota(jnp.int32, (head_width, head_width), 1)
@@ -843,15 +938,33 @@
                     chain_copy(r).start()
 
     chain_point(0, 0)
-    for d in range(3, n_sp):
-        relay(GLU, d)
-    relay(QUERY, 1)
-    relay(OPEN, 2)
-    for d in range(3, n_sp):
-        relay(OPEN, d)
-
-    def gated(first, count):
-        x = dot(nt[first * length:(first + count) * length, :], wab[...])
+    pass_z(6)
+    relay(QUERY, 1, "inner")
+    add_near = adder(acc_ab, wab, 0, 2)
+    add_query = adder(acc_q, wq, 0, 2)
+    drain(GLU, 1)
+    drain(OPEN, 1)
+
+    @pl.when(inner)
+    def _():
+        add_near(sp, True)
+
+    pass_z(7)
+    for c in range(4):
+        pass_far(c)
+    neighbours(GLU, 1, add_near)
+    relay(QUERY, 1, "edge", (0,))
+    pass_far(4)
+    chain_point(1, 1)
+    relay(QUERY, 1, "edge", (1,))
+    pass_far(5)
+    for d in range(2, n_sp - 1):
+        for w in (GLU, OPEN):
+            relay(w, d)
+            drain(w, d)
+        neighbours(GLU, d, add_near)
+
+    def gated(x):
         return (x[:, :channels] * jax.nn.sigmoid(x[:, channels:])).astype(BF16)
 
     def owner(j):
@@ -864,62 +977,71 @@
         return remote(main_in.at[h], main_in.at[h], main_send.at[0], main_recv.at[h], grp=other)
 
     def far_copy(j):
-        return remote(gend.at[j], main_in.at[grp], far_send.at[j], main_recv.at[grp], sp=helped, grp=owner(j))
+        return remote(gend.at[j], main_in.at[grp], far_send.at[0], main_recv.at[grp], sp=helped, grp=owner(j))
 
     def edge_copy(side, j):
         start = length - HALO if side == 0 else 0
         src = main_in.at[grp, pl.ds(start, HALO)] if j == 0 else gout.at[pl.ds(start, HALO)]
         return remote(
-            src, edge_in.at[side, grp], edge_send.at[side, j], edge_recv.at[side, grp],
+            src, edge_in.at[side, grp], edge_send.at[0], edge_recv.at[side, grp],
             sp=sp + 1 if side == 0 else sp - 1, grp=owner(j),
         )
 
     def rim_copy(side):
         start = length - HALO if side == 0 else 0
         return remote(
-            gend.at[1, pl.ds(start, HALO)], edge_in.at[side, grp], rim_send.at[side], edge_recv.at[side, grp], grp=other
+            gend.at[1, pl.ds(start, HALO)], edge_in.at[side, grp], rim_send.at[0], edge_recv.at[side, grp], grp=other
         )
 
     def edge_arrival(side, h):
         place = edge_in.at[side, h]
-        return remote(place, place, edge_send.at[side, 0], edge_recv.at[side, h], grp=other)
+        return remote(place, place, edge_send.at[0], edge_recv.at[side, h], grp=other)
 
     @pl.when(inner)
     def _():
-        own[GLU].wait()
-        own[OPEN].wait()
-
-        @pl.when(helps)
-        def _():
-            for c in range(pieces):
-                tok_f_arrival(2, c).wait_recv()
-                tok_f_arrival(3, c).wait_recv()
-            far = gated(2, 2)
-            gend[0] = far[:length]
-            gend[1] = far[length:]
-            for j in range(2):
-                far_copy(j).start()
-            for side, at in ((0, 1), (1, n_sp - 2)):
-                @pl.when(sp == at)
-                def _(side=side):
-                    rim_copy(side).start()
-                    start = length - HALO if side == 0 else 0
-                    edge_in[side, grp] = gend[0, start:start + HALO, :]
-
-        near = gated(0, 2)
-        main_in[grp] = near[:length]
-        gout[...] = near[length:]
+        near_rows = gated(acc_ab[...])
+        main_in[grp] = near_rows[:length]
+        gout[...] = near_rows[length:]
         main_y().start()
         for side in range(2):
             for j in range(2):
                 edge_copy(side, j).start()
 
-    chain_point(1, 1)
-    relay(QUERY, 2)
-    for at in range(2, n_sp - 1):
-        chain_point(at, at)
-        relay(QUERY, at + 1)
-    chain_point(n_sp - 1, n_sp - 1)
+    def give_far(j):
+        gend[j] = gated(dot(nt[(2 + j) * length:(3 + j) * length, :], wab[...]))
+        far_copy(j).start()
+
+    @pl.when(helps)
+    def _():
+        tok_f_arrival(2).wait_recv()
+        give_far(0)
+        for side, at in ((0, 1), (1, n_sp - 2)):
+            @pl.when(sp == at)
+            def _(side=side):
+                start = length - HALO if side == 0 else 0
+                edge_in[side, grp] = gend[0, start:start + HALO, :]
+
+    pass_far(6)
+    pass_far(7)
+
+    @pl.when(helps)
+    def _():
+        tok_f_arrival(3).wait_recv()
+        give_far(1)
+        for side, at in ((0, 1), (1, n_sp - 2)):
+            @pl.when(sp == at)
+            def _(side=side):
+                rim_copy(side).start()
+
+    for d in range(2, n_sp - 1):
+        chain_point(d, d)
+        relay(QUERY, d)
+    drain(QUERY, 1)
+    add_query(sp, True)
+    neighbours(QUERY, 1, add_query)
+    for d in range(2, n_sp - 1):
+        drain(QUERY, d)
+        neighbours(QUERY, d, add_query)
 
     for h in range(2):
         @pl.when(~(inner & (grp == h)))
@@ -962,16 +1084,78 @@
 
     def stat_copy(step):
         return remote(
-            stat_out, stat_in.at[step], stat_send.at[step], stat_recv.at[step], tp=lax.rem(tp + step + 1, n_tp)
+            stat_out, stat_in.at[step], stat_send.at[0], stat_recv.at[0], tp=lax.rem(tp + step + 1, n_tp)
         )
 
     for step in range(n_tp - 1):
         stat_copy(step).start()
 
-    own[QUERY].wait()
-    query_proj = silu(dot(nt[0:both, :], wq[...]))
-    for u, (j, h) in enumerate(units):
-        query = query_proj[j * length:(j + 1) * length, h * head_width:(h + 1) * head_width]
+    def chip_at(q):
+        return lax.rem(chip + q, chips)
+
+    def chip_back(q):
+        return lax.rem(chip + chips - q, chips)
+
+    def dg_copy(a, q):
+        src = dall.at[tp, grp] if a == 0 else dm_out
+        where = {"tp": chip_at(q) * 2 + core}
+        if a:
+            where["grp"] = other
+        return remote(src, dall.at[tp, grp], dg_send.at[a], dg_recv.at[a, q], **where)
+
+    def d_block(a, q, side):
+        return dall.at[chip_back(q) * 2 + side, other if a else grp]
+
+    def dg_arrival(a, q):
+        place = d_block(a, q, core)
+        return remote(place, place, dg_send.at[a], dg_recv.at[a, q], tp=sibling)
+
+    def df_copy(a, q):
+        place = d_block(a, q, core)
+        return remote(place, place, df_send.at[0], df_recv.at[q], tp=sibling)
+
+    def df_arrival(q):
+        place = dall.at[chip_back(q) * 2 + 1 - core]
+        return remote(place, place, df_send.at[0], df_recv.at[q], tp=sibling)
+
+    def cg_copy(q):
+        return remote(call.at[tp], call.at[tp], cg_send.at[0], cg_recv.at[q], tp=chip_at(q) * 2 + core)
+
+    def cg_arrival(q):
+        place = call.at[chip_back(q) * 2 + core]
+        return remote(place, place, cg_send.at[0], cg_recv.at[q], tp=sibling)
+
+    def cf_copy(q, arriving=False):
+        place = call.at[chip_back(q) * 2 + (1 - core if arriving else core)]
+        return remote(place, place, cf_send.at[0], cf_recv.at[q], tp=sibling)
+
+    chain_point(n_sp - 1, n_sp - 1)
+    stats = stat_out[0:2, :]
+    stat_all = remote(stat_in, stat_in, stat_send.at[0], stat_recv.at[0], tp=sibling)
+    stat_all.wait_recv()
+    for step in range(n_tp - 1):
+        stats = stats + stat_in[step, 0:2, :]
+    center = jnp.sum(jnp.where(same, stats[0:1, :], 0.0), axis=1, keepdims=True) / conv_total
+    squares = jnp.sum(jnp.where(same, stats[1:2, :], 0.0), axis=1, keepdims=True) / conv_total
+    spread = squares - center * center
+    normal = (conv[...] - center) * lax.rsqrt(spread + EPSILON)
+    call[tp] = silu(normal * ng[...] + ns[...]).astype(BF16)
+    for q in range(1, chips):
+        cg_copy(q).start()
+    cf_copy(0).start()
+
+    def delta_term(t):
+        return dot(jnp.concatenate([dall[t, 0], dall[t, 1]], axis=1), odg[t], NT)
+
+    def conv_term(t):
+        return dot(call[t], ocg[t], NT)
+
+    drain(QUERY, n_sp - 1)
+    neighbours(QUERY, n_sp - 1, add_query)
+
+    def read(u):
+        j, h = units[u]
+        query = silu(acc_q[j * length:(j + 1) * length, h * head_width:(h + 1) * head_width])
         query = unit_rows(query) * head_width ** -0.5
         scores = bdot(query, keys[u], NT)
         for r in range(2):
@@ -988,125 +1172,77 @@
         scale = lax.rsqrt(jnp.mean(joined * joined, axis=-1, keepdims=True) + EPSILON)
         return (joined * scale * hgain[...]).astype(BF16)
 
-    def chip_at(q):
-        return lax.rem(chip + q, chips)
-
-    def chip_back(q):
-        return lax.rem(chip + chips - q, chips)
-
-    def dg_copy(a, q):
-        src = dall.at[tp, grp] if a == 0 else dm_out
-        where = {"tp": chip_at(q) * 2 + core}
-        if a:
-            where["grp"] = other
-        return remote(src, dall.at[tp, grp], dg_send.at[a, q], dg_recv.at[a, q], **where)
-
-    def d_block(a, q, side):
-        return dall.at[chip_back(q) * 2 + side, other if a else grp]
-
-    def dg_arrival(a, q):
-        place = d_block(a, q, core)
-        return remote(place, place, dg_send.at[a, q], dg_recv.at[a, q], tp=sibling)
-
-    def df_copy(a, q, arriving=False):
-        place = d_block(a, q, 1 - core if arriving else core)
-        return remote(place, place, df_send.at[a, q], df_recv.at[a, q], tp=sibling)
-
-    def cg_copy(q):
-        return remote(call.at[tp], call.at[tp], cg_send.at[q], cg_recv.at[q], tp=chip_at(q) * 2 + core)
-
-    def cg_arrival(q):
-        place = call.at[chip_back(q) * 2 + core]
-        return remote(place, place, cg_send.at[q], cg_recv.at[q], tp=sibling)
-
-    def cf_copy(q, arriving=False):
-        place = call.at[chip_back(q) * 2 + (1 - core if arriving else core)]
-        return remote(place, place, cf_send.at[q], cf_recv.at[q], tp=sibling)
-
     direct = [(a, q) for q in range(chips) for a in (1, 0) if (a, q) != (0, 0)]
 
     for h in range(heads):
+        read(heads + h)
         dm_out[:, h * head_width:(h + 1) * head_width] = mixed_head(heads + h)
     for q in range(chips - 1, -1, -1):
         dg_copy(1, q).start()
     for h in range(heads):
+        read(h)
         dall[tp, grp, :, h * head_width:(h + 1) * head_width] = mixed_head(h)
     for q in range(1, chips):
         dg_copy(0, q).start()
     df_copy(0, 0).start()
 
-    stats = stat_out[0:2, :]
-    for step in range(n_tp - 1):
-        stat_copy(step).wait_recv()
-        stats = stats + stat_in[step, 0:2, :]
-    center = jnp.sum(jnp.where(same, stats[0:1, :], 0.0), axis=1, keepdims=True) / conv_total
-    squares = jnp.sum(jnp.where(same, stats[1:2, :], 0.0), axis=1, keepdims=True) / conv_total
-    spread = squares - center * center
-    normal = (conv[...] - center) * lax.rsqrt(spread + EPSILON)
-    call[tp] = silu(normal * ng[...] + ns[...]).astype(BF16)
-    for q in range(1, chips):
-        cg_copy(q).start()
-    cf_copy(0).start()
-
     for m in range(2):
-        for step in range(n_tp - 1):
-            od_arrival(m, step).wait_recv()
+        od_all(m).wait_recv()
     load_od.wait()
     load_oc.wait()
-
+    result = conv_term(tp)
+    for q in range(1, chips):
+        cg_arrival(q).wait_recv()
+        cf_copy(q).start()
+    for q in range(1, chips):
+        result = result + conv_term(chip_back(q) * 2 + core)
     for a, q in direct:
         dg_arrival(a, q).wait_recv()
         df_copy(a, q).start()
+        if (a, q) == (1, 0):
+            for p in range(chips):
+                cf_copy(p, True).wait_recv()
+                result = result + conv_term(chip_back(p) * 2 + 1 - core)
+            result = result + delta_term(tp)
     for q in range(1, chips):
-        cg_arrival(q).wait_recv()
-        cf_copy(q).start()
-
-    def delta_term(t):
-        return dot(jnp.concatenate([dall[t, 0], dall[t, 1]], axis=1), odg[t], NT)
-
-    def conv_term(t):
-        return dot(call[t], ocg[t], NT)
-
-    result = delta_term(tp)
+        result = result + delta_term(chip_back(q) * 2 + core)
     for q in range(chips):
-        t = chip_back(q) * 2 + core
-        if q:
-            result = result + delta_term(t)
-        result = result + conv_term(t)
-    for q in range(chips):
-        t = chip_back(q) * 2 + 1 - core
-        df_copy(0, q, True).wait_recv()
-        df_copy(1, q, True).wait_recv()
-        result = result + delta_term(t)
-    for q in range(chips):
-        t = chip_back(q) * 2 + 1 - core
-        cf_copy(q, True).wait_recv()
-        result = result + conv_term(t)
+        df_arrival(q).wait_recv()
+        result = result + delta_term(chip_back(q) * 2 + 1 - core)
     out[...] = result.astype(BF16)
 
-    for w in range(6):
-        for d in range(1, n_sp):
-            for side in range(2):
-                @pl.when(leaves(w, side, d))
-                def _(w=w, d=d, side=side):
-                    z_copy(w, side, d).wait_send()
-    for c in range(pieces):
-        tok_y(0, c).wait_send()
-        tok_f(1, c).wait_send()
-
-        @pl.when(edge)
-        def _(c=c):
-            tok_z(c).wait_send()
-
-        @pl.when(helps)
-        def _(c=c):
-            tok_y(1, c).wait_send()
-            tok_f(2, c).wait_send()
-            tok_f(3, c).wait_send()
+    for side in range(2):
+        for q in range(n_sp):
+            far = n_sp - 1 if side == 0 else 0
+            copies = 0 if q == far else (q + 1 if side == 0 else n_sp - q)
+            wide_to = n_sp - 2 if side == 0 else 1
+            wide_copies = copies if (q < wide_to if side == 0 else q > wide_to) else 0
+            if copies:
+                @pl.when(sp == q)
+                def _(side=side, copies=copies, wide_copies=wide_copies):
+                    place = wg.at[pl.ds(0, copies)]
+                    remote(place, place, g_send.at[side], g_send.at[side], tp=sibling).wait_send()
+                    total = (3 * cols * copies + 2 * channels * wide_copies) * rows // width
+                    place = nt.at[pl.ds(0, total)]
+                    remote(place, place, z_send.at[side], z_send.at[side], tp=sibling).wait_send()
+    half_rows(ty_send.at[0]).wait_send()
+    half_rows(tf_send.at[0]).wait_send()
+
+    @pl.when(edge)
+    def _():
+        half_rows(tz_send.at[0]).wait_send()
+
+    @pl.when(helps)
+    def _():
+        half_rows(ty_send.at[1]).wait_send()
+        half_rows(tf_send.at[1]).wait_send()
+        half_rows(tf_send.at[2]).wait_send()
+        remote(gend, gend, far_send.at[0], far_send.at[0], tp=sibling).wait_send()
+        rim_copy(0).wait_send()
+
     ld_copy.wait_send()
     for m in range(2):
-        for step in range(n_tp - 1):
-            od_copy(m, step).wait_send()
+        od_all(m).wait_send()
     for r in range(2):
         @pl.when(place_of(r) < n_sp - 1)
         def _(r=r):
@@ -1115,28 +1251,20 @@
     @pl.when(inner)
     def _():
         main_y().wait_send()
-        for side in range(2):
-            for j in range(2):
-                edge_copy(side, j).wait_send()
-
-    @pl.when(helps)
-    def _():
-        for j in range(2):
-            far_copy(j).wait_send()
-    for side, at in ((0, 1), (1, n_sp - 2)):
-        @pl.when(sp == at)
-        def _(side=side):
-            rim_copy(side).wait_send()
-    for step in range(n_tp - 1):
-        stat_copy(step).wait_send()
-    df_copy(0, 0).wait_send()
-    for a, q in direct:
-        dg_copy(a, q).wait_send()
-        df_copy(a, q).wait_send()
-    for q in range(chips):
-        if q:
-            cg_copy(q).wait_send()
-        cf_copy(q).wait_send()
+        remote(edge_in, edge_in, edge_send.at[0], edge_send.at[0], tp=sibling).wait_send()
+
+    stat_all.wait_send()
+    place = dall.at[pl.ds(0, chips), 0]
+    remote(place, place, dg_send.at[1], dg_send.at[1], tp=sibling).wait_send()
+    if chips > 1:
+        place = dall.at[pl.ds(0, chips - 1), 0]
+        remote(place, place, dg_send.at[0], dg_send.at[0], tp=sibling).wait_send()
+        place = call.at[pl.ds(0, chips - 1)]
+        remote(place, place, cg_send.at[0], cg_send.at[0], tp=sibling).wait_send()
+    place = dall.at[pl.ds(0, chips)]
+    remote(place, place, df_send.at[0], df_send.at[0], tp=sibling).wait_send()
+    place = call.at[pl.ds(0, chips)]
+    remote(place, place, cf_send.at[0], cf_send.at[0], tp=sibling).wait_send()
 
 
 def solution(mesh):
@@ -1156,10 +1284,12 @@
         dma, vmem = pltpu.SemaphoreType.DMA, pltpu.VMEM
         anywhere = pl.BlockSpec(memory_space=pltpu.HBM)
         inside = pl.BlockSpec(memory_space=pltpu.VMEM)
-        if n_grp == 2 and n_sp >= 4 and n_tp % 2 == 0 and heads % 2 == 0 and channels % 256 == 0:
+        if n_grp == 2 and n_sp >= 4 and n_tp % 2 == 0 and heads % 2 == 0 and channels % 256 == 0                 and (3 * head_cols + 2 * channels) * rows * n_sp <= 8 * length * width:
             cols, ch, chips, steps = head_cols // 2, channels // 2, n_tp // 2, n_tp - 1
             pieces = 4
             scratch = [
+                vmem((1, width), F32), vmem((pairs, length), F32), vmem((1, head_width), F32),
+                vmem(conv_kernel.shape, F32), vmem((1, channels), F32), vmem((1, channels), F32),
                 vmem((length, width), BF16), vmem((4 * length, width), BF16),
                 vmem((width, cols), BF16), vmem((width, cols), BF16), vmem((width, cols), BF16),
                 vmem((width, 2 * ch), BF16), vmem((n_sp, 4 * heads, rows), BF16),
@@ -1177,25 +1307,26 @@
                 vmem((2, length + 2 * HALO, ch), F32), vmem((length, channels), F32),
                 vmem((8, length), F32), vmem((steps, 8, length), F32),
                 vmem((n_tp, 2, length, cols), BF16), vmem((length, cols), BF16),
-                vmem((n_tp, length, channels), BF16),
-                dma((9,)),
-                dma((6, 2, n_sp - 1)), dma((6, 2, n_sp - 1)),
-                dma((2, pieces)), dma((2, pieces)), dma((3, pieces)), dma((3, pieces)),
-                dma((pieces,)), dma((pieces,)),
-                dma((1,)), dma((1,)), dma((2, steps)), dma((2, steps)), dma((2,)), dma((2,)),
-                dma((1,)), dma((2,)), dma((2, 2)), dma((2, 2)), dma((2,)), dma((2,)),
-                dma((steps,)), dma((steps,)),
-                dma((2, chips)), dma((2, chips)), dma((2, chips)), dma((2, chips)),
-                dma((chips,)), dma((chips,)), dma((chips,)), dma((chips,)),
+                vmem((n_tp, length, channels), BF16), vmem((2 * length, 2 * ch), F32), vmem((2 * length, cols), F32),
+                vmem((2 * length, cols), F32), vmem((2 * length, cols), F32),
+                dma((15,)),
+                dma((2,)), dma((n_sp,)), dma((2,)), dma((n_sp, 12)),
+                dma((2,)), dma((pieces,)), dma((2 * pieces,)), dma((3,)), dma((3,)),
+                dma((1,)), dma((2 * pieces,)),
+                dma((1,)), dma((1,)), dma((2,)), dma((2,)), dma((2,)), dma((2,)),
+                dma((1,)), dma((2,)), dma((1,)), dma((2, 2)), dma((1,)), dma((1,)),
+                dma((1,)), dma((1,)),
+                dma((2,)), dma((2, chips)), dma((1,)), dma((chips,)),
+                dma((1,)), dma((chips,)), dma((1,)), dma((chips,)),
             ]
             return pl.pallas_call(
                 functools.partial(fused, (n_sp, n_tp, float(channels * n_tp))),
-                out_shape=jax.ShapeDtypeStruct((length, columns), BF16),
-                in_specs=[anywhere, inside] + [anywhere] * 6 + [inside] * 5 + [anywhere] * 2,
+                out_shape=pltpu.VMEM((length, columns), BF16),
+                in_specs=[anywhere] * 15,
                 out_specs=inside,
                 scratch_shapes=scratch,
                 compiler_params=pltpu.CompilerParams(
-                    collective_id=0, has_side_effects=True, vmem_limit_bytes=48 * 1024 * 1024
+                    collective_id=0, has_side_effects=True, vmem_limit_bytes=58 * 1024 * 1024
                 ),
             )(
                 tokens_in, input_gain.reshape(1, width), w_key, w_gates.T, w_value, w_query,

time: 77.7 us -> 55.6 us (0.72)
  local copies, waits for them, and re-layouts: 12 us -> 0.71 us
  Pallas kernels: 65.1 us -> 54.5 us
    unnamed x31 -> x1, local copies, waits for them, and re-layouts: 12 us -> 0.71 us
    pallas_call x1, Pallas kernels: 65.1 us -> 54.5 us  [on_device(): pl.pallas_call(functools.partial(fused, (n_sp, n_tp, float(channels * n_t...]
where the time goes in v3:
time: 55.6 us; the launch traced here: 55.3 us
  Pallas kernels  54.5 us (98%)
  local copies, waits for them, and re-layouts  0.71 us (1%)
    pallas_call x1, Pallas kernels, on_device(): pl.pallas_call(functools.partial(fused, (n_sp, n_tp, float(channels * n_t...  54.5 us

profile of v3, /device:TPU:0, one launch (start us, length us, event | category | flops | bytes accessed | tf_op | source)
XLA Modules:
  0.0 55.3 jit_solution(3391507527778686804)
XLA Ops:
  0.0 54.5 %shard_map.145 = bf16[256,512]{1,0:T(8,128)(2,1)S(1)} custom-call(bf16[256,2048]{1,0:T(8,128)(2,1)} %tok_h.1, f32[1,2048]{1,0:T(1,128)} %bitcast.6, bf16[512,256]{1,0:T(8,128)(2,1)} %wk_h.1, bf16[8,512]{1,0:T(8,128)(2,1)} %bitcast.7, bf16[512,256]{1,0:T(8,128)(2,1)} %wv_h.1, bf16[512,256]{1,0:T(8,128)(2,1)} %wq_h.1, bf16[512,256]{1,0:T(8,128)(2,1)} %wa_h.1, ...), custom_call_target="tpu_custom_call" | custom-call | tf_op jit(solution)/shard_map/pallas_call | solution.py:1322
  54.6 0.7 %copy.17 = bf16[256,512]{1,0:T(8,128)(2,1)} copy(bf16[256,512]{1,0:T(8,128)(2,1)S(1)} %shard_map.145) | data formatting | bytes 524288

commit v4 on v3

--- a/solution.py
+++ b/solution.py
@@ -566,7 +566,8 @@
     small = [
         pltpu.make_async_copy(src, dst, local_sem.at[9 + i])
         for i, (src, dst) in enumerate(
-            ((gain_h, gain), (ldt_h, ldt), (hgain_h, hgain), (ck_h, ck), (ng_h, ng), (ns_h, ns))
+            ((gain_h, gain), (ldt_h, ldt), (hgain_h, hgain), (ng_h, ng), (ns_h, ns),
+             (ck_h.at[:, pl.ds(0, channels)], ck.at[0]), (ck_h.at[:, pl.ds(channels, channels)], ck.at[1]))
         )
     ]
     for copy in small:
@@ -734,12 +735,14 @@
         own[w].wait()
     offer(VALUE, edge)
     offer(GLU, edge)
-    offer(OPEN, edge)
-
-    @pl.when(edge)
-    def _():
-        for c in range(grains):
-            tok_z(c).start()
+    for first in (0, grains // 2):
+        @pl.when(edge)
+        def _(first=first):
+            for c in range(first, first + grains // 2):
+                tok_z(c).start()
+
+        if first == 0:
+            offer(OPEN, edge)
 
     offer(QUERY, edge)
     for m in (1, 0):
@@ -812,6 +815,7 @@
     offer(VALUE, inner, (0,))
     relay(KEY, 1, None, (2, 3))
     offer(VALUE, inner, (1,))
+    offer(GLU, inner)
     relay(GATE, 2)
     pass_y(0, 0)
     for d in range(2, n_sp - 1):
@@ -819,7 +823,6 @@
     relay(VALUE, 1, None, (0,))
     for d in range(2, n_sp - 1):
         relay(KEY, d, None, (2, 3))
-    offer(GLU, inner)
     pass_y(0, 1)
     relay(VALUE, 1, None, (1,))
     offer(OPEN, inner)
@@ -845,18 +848,19 @@
         neighbours(KEY, d, add_key[0])
     ld_copy.wait_recv()
     tok_f_arrival(1).wait_recv()
-    relay(OPEN, 1)
+    pass_z(0)
     weights_of(1)
-    pass_z(0)
-    pass_value()
+    pass_z(1)
+    pass_z(2)
     add_key[1](sp, True)
     for d in range(1, n_sp - 1):
         neighbours(KEY, d, add_key[1])
     add_value[1](sp, True)
     neighbours(VALUE, 1, add_value[1])
-    pass_z(1)
+    pass_z(3)
     drain(KEY, n_sp - 1)
     neighbours(KEY, n_sp - 1, adder(acc_k, wk, 0, 2))
+    pass_value()
 
     both = 2 * length
     key_proj = silu(acc_k[...])
@@ -873,8 +877,7 @@
             xinv[p] = jnp.where(same, 1.0, jnp.where(near, -lower, 0.0))
 
     service = {
-        4: [lambda: pass_z(2)],
-        8: [lambda: pass_z(3)],
+        8: [lambda: relay(OPEN, 1)],
         32: [lambda: pass_z(4)],
         128: [lambda: pass_z(5)],
     }
@@ -955,7 +958,6 @@
     neighbours(GLU, 1, add_near)
     relay(QUERY, 1, "edge", (0,))
     pass_far(4)
-    chain_point(1, 1)
     relay(QUERY, 1, "edge", (1,))
     pass_far(5)
     for d in range(2, n_sp - 1):
@@ -1022,6 +1024,7 @@
                 edge_in[side, grp] = gend[0, start:start + HALO, :]
 
     pass_far(6)
+    chain_point(1, 1)
     pass_far(7)
 
     @pl.when(helps)
@@ -1043,39 +1046,40 @@
         drain(QUERY, d)
         neighbours(QUERY, d, add_query)
 
-    for h in range(2):
-        @pl.when(~(inner & (grp == h)))
+    taps = ck.shape[1]
+    for step in range(2):
+        h = grp if step == 0 else other
+        skip = sp < 0 if step else sp >= 0
+
+        @pl.when(edge if step == 0 else sp >= 0)
         def _(h=h):
             main_arrival(h).wait_recv()
 
-        @pl.when((sp > 0) & ~((sp == 1) & (grp == h)))
+        @pl.when((sp > 0) & ~((sp == 1) & skip))
         def _(h=h):
             edge_arrival(0, h).wait_recv()
 
-        @pl.when((sp < n_sp - 1) & ~((sp == n_sp - 2) & (grp == h)))
+        @pl.when((sp < n_sp - 1) & ~((sp == n_sp - 2) & skip))
         def _(h=h):
             edge_arrival(1, h).wait_recv()
 
-        pad[h, HALO:HALO + length, :] = main_in[h].astype(F32)
+        pad[step, HALO:HALO + length, :] = main_in[h].astype(F32)
         for side, start, none in ((0, 0, 0), (1, HALO + length, n_sp - 1)):
             @pl.when(sp != none)
-            def _(h=h, side=side, start=start):
-                pad[h, start:start + HALO, :] = edge_in[side, h].astype(F32)
+            def _(h=h, step=step, side=side, start=start):
+                pad[step, start:start + HALO, :] = edge_in[side, h].astype(F32)
 
             @pl.when(sp == none)
-            def _(h=h, start=start):
-                pad[h, start:start + HALO, :] = jnp.zeros((HALO, channels), F32)
-
-    taps = ck.shape[0]
-    for h in range(2):
-        lanes = slice(h * channels, (h + 1) * channels)
+            def _(step=step, start=start):
+                pad[step, start:start + HALO, :] = jnp.zeros((HALO, channels), F32)
+
         for at in range(0, length, chunk):
             first = at + HALO - taps // 2
-            total = pad[h, first:first + chunk, :] * ck[0:1, lanes]
+            total = pad[step, first:first + chunk, :] * ck[h, 0:1, :]
             for k in range(1, taps):
-                total = total + pad[h, first + k:first + k + chunk, :] * ck[k:k + 1, lanes]
-            conv[at:at + chunk, lanes] = total
-    filtered = conv[...]
+                total = total + pad[step, first + k:first + k + chunk, :] * ck[h, k:k + 1, :]
+            conv[h, at:at + chunk, :] = total
+    filtered = jnp.concatenate([conv[0], conv[1]], axis=1)
     sum_col = jnp.sum(filtered, axis=-1, keepdims=True)
     square_col = jnp.sum(filtered * filtered, axis=-1, keepdims=True)
     stat_out[...] = jnp.zeros(stat_out.shape, F32)
@@ -1129,7 +1133,6 @@
         place = call.at[chip_back(q) * 2 + (1 - core if arriving else core)]
         return remote(place, place, cf_send.at[0], cf_recv.at[q], tp=sibling)
 
-    chain_point(n_sp - 1, n_sp - 1)
     stats = stat_out[0:2, :]
     stat_all = remote(stat_in, stat_in, stat_send.at[0], stat_recv.at[0], tp=sibling)
     stat_all.wait_recv()
@@ -1138,7 +1141,7 @@
     center = jnp.sum(jnp.where(same, stats[0:1, :], 0.0), axis=1, keepdims=True) / conv_total
     squares = jnp.sum(jnp.where(same, stats[1:2, :], 0.0), axis=1, keepdims=True) / conv_total
     spread = squares - center * center
-    normal = (conv[...] - center) * lax.rsqrt(spread + EPSILON)
+    normal = (jnp.concatenate([conv[0], conv[1]], axis=1) - center) * lax.rsqrt(spread + EPSILON)
     call[tp] = silu(normal * ng[...] + ns[...]).astype(BF16)
     for q in range(1, chips):
         cg_copy(q).start()
@@ -1150,6 +1153,7 @@
     def conv_term(t):
         return dot(call[t], ocg[t], NT)
 
+    chain_point(n_sp - 1, n_sp - 1)
     drain(QUERY, n_sp - 1)
     neighbours(QUERY, n_sp - 1, add_query)
 
@@ -1289,7 +1293,7 @@
             pieces = 4
             scratch = [
                 vmem((1, width), F32), vmem((pairs, length), F32), vmem((1, head_width), F32),
-                vmem(conv_kernel.shape, F32), vmem((1, channels), F32), vmem((1, channels), F32),
+                vmem((2, conv_kernel.shape[0], ch), F32), vmem((1, channels), F32), vmem((1, channels), F32),
                 vmem((length, width), BF16), vmem((4 * length, width), BF16),
                 vmem((width, cols), BF16), vmem((width, cols), BF16), vmem((width, cols), BF16),
                 vmem((width, 2 * ch), BF16), vmem((n_sp, 4 * heads, rows), BF16),
@@ -1304,12 +1308,12 @@
                 vmem((2, heads, head_width, head_width), BF16), vmem((2, heads, head_width, head_width), BF16),
                 vmem((length, ch), BF16), vmem((2, length, ch), BF16), vmem((2, length, ch), BF16),
                 vmem((2, 2, HALO, ch), BF16),
-                vmem((2, length + 2 * HALO, ch), F32), vmem((length, channels), F32),
+                vmem((2, length + 2 * HALO, ch), F32), vmem((2, length, ch), F32),
                 vmem((8, length), F32), vmem((steps, 8, length), F32),
                 vmem((n_tp, 2, length, cols), BF16), vmem((length, cols), BF16),
                 vmem((n_tp, length, channels), BF16), vmem((2 * length, 2 * ch), F32), vmem((2 * length, cols), F32),
                 vmem((2 * length, cols), F32), vmem((2 * length, cols), F32),
-                dma((15,)),
+                dma((16,)),
                 dma((2,)), dma((n_sp,)), dma((2,)), dma((n_sp, 12)),
                 dma((2,)), dma((pieces,)), dma((2 * pieces,)), dma((3,)), dma((3,)),
                 dma((1,)), dma((2 * pieces,)),

time: 55.6 us -> 53.1 us (0.955)
  Pallas kernels: 54.5 us -> 52.1 us
    pallas_call x1, Pallas kernels: 54.5 us -> 52.1 us  [on_device(): pl.pallas_call(functools.partial(fused, (n_sp, n_tp, float(channels * n_t...]
where the time goes in v4:
time: 53.1 us; the launch traced here: 52.8 us
  Pallas kernels  52.1 us (98%)
  local copies, waits for them, and re-layouts  0.71 us (1%)
    pallas_call x1, Pallas kernels, on_device(): pl.pallas_call(functools.partial(fused, (n_sp, n_tp, float(channels * n_t...  52.1 us

profile of v4, /device:TPU:0, one launch (start us, length us, event | category | flops | bytes accessed | tf_op | source)
XLA Modules:
  0.0 52.8 jit_solution(7306922614794691781)
XLA Ops:
  0.0 52.1 %shard_map.145 = bf16[256,512]{1,0:T(8,128)(2,1)S(1)} custom-call(bf16[256,2048]{1,0:T(8,128)(2,1)} %tok_h.1, f32[1,2048]{1,0:T(1,128)} %bitcast.6, bf16[512,256]{1,0:T(8,128)(2,1)} %wk_h.1, bf16[8,512]{1,0:T(8,128)(2,1)} %bitcast.7, bf16[512,256]{1,0:T(8,128)(2,1)} %wv_h.1, bf16[512,256]{1,0:T(8,128)(2,1)} %wq_h.1, bf16[512,256]{1,0:T(8,128)(2,1)} %wa_h.1, ...), custom_call_target="tpu_custom_call" | custom-call | tf_op jit(solution)/shard_map/pallas_call | solution.py:1326
  52.1 0.7 %copy.17 = bf16[256,512]{1,0:T(8,128)(2,1)} copy(bf16[256,512]{1,0:T(8,128)(2,1)S(1)} %shard_map.145) | data formatting | bytes 524288

commit v5 on v4

--- a/solution.py
+++ b/solution.py
@@ -486,7 +486,7 @@
           keys, vals, betas, cums, xinv, gaps, rhs, local_out, reads, maps, ends,
           chain_in, chain_out, gout, gend, main_in, edge_in, pad, conv, stat_out, stat_in,
           dall, dm_out, call, acc_ab, acc_q, acc_k, acc_v,
-          local_sem, g_send, g_recv, z_send, z_recv, ty_send, ty_recv, tx_recv, tf_send, tf_recv, tz_send, tz_recv,
+          local_sem, g_send, g_recv, z_send, z_recv, t_send, ty_recv, tx_recv, tf_recv, tz_recv,
           ld_send, ld_recv, od_send, od_recv, chain_send, chain_recv,
           main_send, main_recv, edge_send, edge_recv, far_send, rim_send,
           stat_send, stat_recv, dg_send, dg_recv, df_send, df_recv, cg_send, cg_recv, cf_send, cf_recv):
@@ -519,8 +519,8 @@
             src_ref=src, dst_ref=dst, send_sem=send, recv_sem=recv, device_id=where, device_id_type=MESH
         )
 
-    counts = (4, 1, 2, 2, 2, 2)
-    firsts = (0, 0, 4, 6, 8, 10)
+    counts = (4, 1, 2, 2, 1, 1)
+    firsts = (0, 0, 4, 6, 8, 9)
 
     def source(w):
         if w == GATE:
@@ -619,13 +619,15 @@
     def origin(side, d):
         return sp - d if side == 0 else sp + d
 
-    def z_block(w, index, side, k):
+    def z_block(w, index, side, k, here=False):
+        ahead = sp + 1 if side == 0 else sp - 1
         place = target(w, index, k)
+        slot = jnp.where(index > (sp if here else ahead), index - 1, index)
         if w == GATE:
-            send, recv = g_send.at[side], g_recv.at[index]
+            send, recv = g_send.at[side], g_recv.at[slot]
         else:
-            send, recv = z_send.at[side], z_recv.at[index, firsts[w] + k]
-        return remote(place, place, send, recv, sp=sp + 1 if side == 0 else sp - 1)
+            send, recv = z_send.at[side], z_recv.at[slot, firsts[w] + k]
+        return remote(place, place, send, recv, sp=ahead)
 
     def cuts(w):
         return range(counts[w])
@@ -654,7 +656,7 @@
 
                 @pl.when(here)
                 def _(side=side, k=k):
-                    z_block(w, origin(side, d), side, k).wait_recv()
+                    z_block(w, origin(side, d), side, k, True).wait_recv()
                     z_block(w, origin(side, d), side, k).start()
 
     def drain(w, d):
@@ -664,7 +666,7 @@
 
                 @pl.when(arrives(w, side, d) & ~onward)
                 def _(side=side, k=k):
-                    z_block(w, origin(side, d), side, k).wait_recv()
+                    z_block(w, origin(side, d), side, k, True).wait_recv()
 
     pieces = ty_recv.shape[0]
     half = length // 2
@@ -678,25 +680,25 @@
 
     def tok_y(k, c):
         return remote(
-            part(2 * k, core, c), part(2 * k + 1, core, c), ty_send.at[k], (ty_recv, tx_recv)[k].at[c], grp=other
+            part(2 * k, core, c), part(2 * k + 1, core, c), t_send.at[0], (ty_recv, tx_recv)[k].at[c], grp=other
         )
 
     def tok_z(c):
         src = nt.at[pl.ds(pl.multiple_of(core * half + c * grain, 16), grain)]
-        return remote(src, part(2, core, c), tz_send.at[0], tz_recv.at[c], sp=helper)
+        return remote(src, part(2, core, c), t_send.at[0], tz_recv.at[c], sp=helper)
 
     def tok_f(block, c):
         return remote(
-            part(block, core, c), part(block, core, c), tf_send.at[block - 1], tf_recv.at[block - 1], tp=sibling
+            part(block, core, c), part(block, core, c), t_send.at[0], tf_recv.at[block - 1], tp=sibling
         )
 
     def tok_f_arrival(block):
         place = nt.at[pl.ds(pl.multiple_of(block * length + (1 - core) * half, 16), half)]
-        return remote(place, place, tf_send.at[block - 1], tf_recv.at[block - 1], tp=sibling)
-
-    def half_rows(send):
-        place = nt.at[pl.ds(0, half)]
-        return remote(place, place, send, send, tp=sibling)
+        return remote(place, place, t_send.at[0], tf_recv.at[block - 1], tp=sibling)
+
+    def sent_rows(count):
+        place = nt.at[pl.ds(0, count * half)]
+        return remote(place, place, t_send.at[0], t_send.at[0], tp=sibling)
 
     def pass_y(k, c):
         tok_y(k, c).wait_recv()
@@ -1037,8 +1039,8 @@
                 rim_copy(side).start()
 
     for d in range(2, n_sp - 1):
+        relay(QUERY, d)
         chain_point(d, d)
-        relay(QUERY, d)
     drain(QUERY, 1)
     add_query(sp, True)
     neighbours(QUERY, 1, add_query)
@@ -1153,7 +1155,6 @@
     def conv_term(t):
         return dot(call[t], ocg[t], NT)
 
-    chain_point(n_sp - 1, n_sp - 1)
     drain(QUERY, n_sp - 1)
     neighbours(QUERY, n_sp - 1, add_query)
 
@@ -1178,13 +1179,14 @@
 
     direct = [(a, q) for q in range(chips) for a in (1, 0) if (a, q) != (0, 0)]
 
+    for u in range(n_units):
+        read(u)
+    chain_point(n_sp - 1, n_sp - 1)
     for h in range(heads):
-        read(heads + h)
         dm_out[:, h * head_width:(h + 1) * head_width] = mixed_head(heads + h)
     for q in range(chips - 1, -1, -1):
         dg_copy(1, q).start()
     for h in range(heads):
-        read(h)
         dall[tp, grp, :, h * head_width:(h + 1) * head_width] = mixed_head(h)
     for q in range(1, chips):
         dg_copy(0, q).start()
@@ -1229,18 +1231,17 @@
                     total = (3 * cols * copies + 2 * channels * wide_copies) * rows // width
                     place = nt.at[pl.ds(0, total)]
                     remote(place, place, z_send.at[side], z_send.at[side], tp=sibling).wait_send()
-    half_rows(ty_send.at[0]).wait_send()
-    half_rows(tf_send.at[0]).wait_send()
-
     @pl.when(edge)
     def _():
-        half_rows(tz_send.at[0]).wait_send()
+        sent_rows(3).wait_send()
+
+    @pl.when(inner & ~helps)
+    def _():
+        sent_rows(2).wait_send()
 
     @pl.when(helps)
     def _():
-        half_rows(ty_send.at[1]).wait_send()
-        half_rows(tf_send.at[1]).wait_send()
-        half_rows(tf_send.at[2]).wait_send()
+        sent_rows(5).wait_send()
         remote(gend, gend, far_send.at[0], far_send.at[0], tp=sibling).wait_send()
         rim_copy(0).wait_send()
 
@@ -1314,9 +1315,8 @@
                 vmem((n_tp, length, channels), BF16), vmem((2 * length, 2 * ch), F32), vmem((2 * length, cols), F32),
                 vmem((2 * length, cols), F32), vmem((2 * length, cols), F32),
                 dma((16,)),
-                dma((2,)), dma((n_sp,)), dma((2,)), dma((n_sp, 12)),
-                dma((2,)), dma((pieces,)), dma((2 * pieces,)), dma((3,)), dma((3,)),
-                dma((1,)), dma((2 * pieces,)),
+                dma((2,)), dma((n_sp - 1,)), dma((2,)), dma((n_sp - 1, 10)),
+                dma((1,)), dma((pieces,)), dma((2 * pieces,)), dma((3,)), dma((2 * pieces,)),
                 dma((1,)), dma((1,)), dma((2,)), dma((2,)), dma((2,)), dma((2,)),
                 dma((1,)), dma((2,)), dma((1,)), dma((2, 2)), dma((1,)), dma((1,)),
                 dma((1,)), dma((1,)),

time: 53.1 us -> 52.8 us (level)
  no operation moved by 1% of the time
where the time goes in v5:
time: 52.8 us; the launch traced here: 52.5 us
  Pallas kernels  51.8 us (98%)
  local copies, waits for them, and re-layouts  0.71 us (1%)
    pallas_call x1, Pallas kernels, on_device(): pl.pallas_call(functools.partial(fused, (n_sp, n_tp, float(channels * n_t...  51.8 us

profile of v5, /device:TPU:0, one launch (start us, length us, event | category | flops | bytes accessed | tf_op | source)
XLA Modules:
  0.0 52.5 jit_solution(14994468066869082835)
XLA Ops:
  0.0 51.8 %shard_map.145 = bf16[256,512]{1,0:T(8,128)(2,1)S(1)} custom-call(bf16[256,2048]{1,0:T(8,128)(2,1)} %tok_h.1, f32[1,2048]{1,0:T(1,128)} %bitcast.6, bf16[512,256]{1,0:T(8,128)(2,1)} %wk_h.1, bf16[8,512]{1,0:T(8,128)(2,1)} %bitcast.7, bf16[512,256]{1,0:T(8,128)(2,1)} %wv_h.1, bf16[512,256]{1,0:T(8,128)(2,1)} %wq_h.1, bf16[512,256]{1,0:T(8,128)(2,1)} %wa_h.1, ...), custom_call_target="tpu_custom_call" | custom-call | tf_op jit(solution)/shard_map/pallas_call | solution.py:1326
  51.8 0.7 %copy.17 = bf16[256,512]{1,0:T(8,128)(2,1)} copy(bf16[256,512]{1,0:T(8,128)(2,1)S(1)} %shard_map.145) | data formatting | bytes 524288

commit v6 on v5

--- a/solution.py
+++ b/solution.py
@@ -689,12 +689,18 @@
 
     def tok_f(block, c):
         return remote(
-            part(block, core, c), part(block, core, c), t_send.at[0], tf_recv.at[block - 1], tp=sibling
+            part(block, core, c), part(block, core, c), t_send.at[0],
+            tf_recv.at[3 if block == 3 and c >= grains // 2 else block - 1], tp=sibling
         )
 
     def tok_f_arrival(block):
         place = nt.at[pl.ds(pl.multiple_of(block * length + (1 - core) * half, 16), half)]
         return remote(place, place, t_send.at[0], tf_recv.at[block - 1], tp=sibling)
+
+    def tok_late(k):
+        start = 3 * length + (1 - core) * half + k * (half // 2)
+        place = nt.at[pl.ds(pl.multiple_of(start, 16), half // 2)]
+        return remote(place, place, t_send.at[0], tf_recv.at[2 + k], tp=sibling)
 
     def sent_rows(count):
         place = nt.at[pl.ds(0, count * half)]
@@ -1015,10 +1021,25 @@
         gend[j] = gated(dot(nt[(2 + j) * length:(3 + j) * length, :], wab[...]))
         far_copy(j).start()
 
+    def give_late(k):
+        tok_late(k).wait_recv()
+        size = half // 2
+        spots = (k * size, half + k * size)
+        x = jnp.concatenate([nt[3 * length + at:3 * length + at + size, :] for at in spots], axis=0)
+        late = gated(dot(x, wab[...]))
+        for i, at in enumerate(spots):
+            gend[1, at:at + size, :] = late[i * size:(i + 1) * size]
+        for at in spots:
+            remote(
+                gend.at[1, pl.ds(at, size)], main_in.at[grp, pl.ds(at, size)],
+                far_send.at[0], main_recv.at[grp], sp=helped, grp=other,
+            ).start()
+
     @pl.when(helps)
     def _():
         tok_f_arrival(2).wait_recv()
         give_far(0)
+        give_late(0)
         for side, at in ((0, 1), (1, n_sp - 2)):
             @pl.when(sp == at)
             def _(side=side):
@@ -1031,8 +1052,7 @@
 
     @pl.when(helps)
     def _():
-        tok_f_arrival(3).wait_recv()
-        give_far(1)
+        give_late(1)
         for side, at in ((0, 1), (1, n_sp - 2)):
             @pl.when(sp == at)
             def _(side=side):
@@ -1316,7 +1336,7 @@
                 vmem((2 * length, cols), F32), vmem((2 * length, cols), F32),
                 dma((16,)),
                 dma((2,)), dma((n_sp - 1,)), dma((2,)), dma((n_sp - 1, 10)),
-                dma((1,)), dma((pieces,)), dma((2 * pieces,)), dma((3,)), dma((2 * pieces,)),
+                dma((1,)), dma((pieces,)), dma((2 * pieces,)), dma((4,)), dma((2 * pieces,)),
                 dma((1,)), dma((1,)), dma((2,)), dma((2,)), dma((2,)), dma((2,)),
                 dma((1,)), dma((2,)), dma((1,)), dma((2, 2)), dma((1,)), dma((1,)),
                 dma((1,)), dma((1,)),

time: 52.8 us -> 52.9 us (level)
  the two profiles are of different devices: /device:TPU:0 before, /device:TPU:9 now
where the time goes in v6:
time: 52.9 us; the launch traced here: 52.7 us
  Pallas kernels  52 us (98%)
  local copies, waits for them, and re-layouts  0.71 us (1%)
    pallas_call x1, Pallas kernels, on_device(): pl.pallas_call(functools.partial(fused, (n_sp, n_tp, float(channels * n_t...  52 us

profile of v6, /device:TPU:9, one launch (start us, length us, event | category | flops | bytes accessed | tf_op | source)
XLA Modules:
  0.0 52.7 jit_solution(15963385237635740337)
XLA Ops:
  0.0 52.0 %shard_map.145 = bf16[256,512]{1,0:T(8,128)(2,1)S(1)} custom-call(bf16[256,2048]{1,0:T(8,128)(2,1)} %tok_h.1, f32[1,2048]{1,0:T(1,128)} %bitcast.6, bf16[512,256]{1,0:T(8,128)(2,1)} %wk_h.1, bf16[8,512]{1,0:T(8,128)(2,1)} %bitcast.7, bf16[512,256]{1,0:T(8,128)(2,1)} %wv_h.1, bf16[512,256]{1,0:T(8,128)(2,1)} %wq_h.1, bf16[512,256]{1,0:T(8,128)(2,1)} %wa_h.1, ...), custom_call_target="tpu_custom_call" | custom-call | tf_op jit(solution)/shard_map/pallas_call | solution.py:1346
  52.0 0.7 %copy.17 = bf16[256,512]{1,0:T(8,128)(2,1)} copy(bf16[256,512]{1,0:T(8,128)(2,1)S(1)} %shard_map.145) | data formatting | bytes 524288
